TPU v7x, 256 devices: a whole 4x4x8 slice. The times are simulated.
256 devices in a mesh: sp: 64 (over z, x, core), tp: 4 (over y).
Axes of the slice: x: 4, y: 4, z: 8, core: 2. Of those that a mesh axis runs over, the one named last changes fastest.
Arguments:
- resid: bfloat16 [16384, 2048], P(('sp', 'tp')), may hold values from -6 to 6
- query_wide: bfloat16 [16384, 768], P('sp', 'tp'), may hold values from -2000 to 2000
- query_narrow: bfloat16 [16384, 512], P('sp', 'tp'), may hold values from -2000 to 2000
- latent: bfloat16 [16384, 256], P('sp'), may hold values from -6 to 6
- rope_key: bfloat16 [16384, 64], P('sp'), may hold values from -6 to 6
- latent_gain: float32 [256], replicated, may hold values from 0.1 to 1.9
- key_up_wide: bfloat16 [256, 512], replicated, may hold values from -0.375 to 0.375
- value_up_wide: bfloat16 [256, 512], replicated, may hold values from -0.375 to 0.375
- key_up_narrow: bfloat16 [256, 256], replicated, may hold values from -0.375 to 0.375
- value_up_narrow: bfloat16 [256, 256], replicated, may hold values from -0.375 to 0.375
- out_wide: bfloat16 [512, 2048], P('tp'), may hold values from -0.21875 to 0.21875
- out_narrow: bfloat16 [256, 2048], P('tp'), may hold values from -0.21875 to 0.21875
- attn_gain: float32 [2048], replicated, may hold values from 0.1 to 1.9
- ffn_gain: float32 [2048], replicated, may hold values from 0.1 to 1.9
- moe_gain: float32 [2048], replicated, may hold values from 0.1 to 1.9
- routes: int32 [16384, 2], P(('sp', 'tp')), may hold values from 0 to 63, all different within a row; in each aligned block of 64 rows (0 to 63, 64 to 127, ...) at most 3 rows name the same one
- route_logit: float32 [16384, 2], P(('sp', 'tp')), may hold values from -8 to 8
- expert_gate: bfloat16 [64, 2048, 3584], P('sp', None, 'tp'), may hold values from -0.125 to 0.125
- expert_up: bfloat16 [64, 2048, 3584], P('sp', None, 'tp'), may hold values from -0.125 to 0.125
- expert_down: bfloat16 [64, 3584, 2048], P('sp', 'tp'), may hold values from -0.09375 to 0.09375
Outputs:
- mixed: bfloat16 [16384, 2048], P(('sp', 'tp'))
Inputs may be any that keep to these rules, and one draw needn't show every extreme that they name: `routes`: in each aligned block of 64 rows no expert is named by more than 3 rows, and a row's experts differ.
All inputs are finite; a program needn't handle non-finite values.
Results may differ from a plain program's by a relative error of at most 0.033.
Values may be sent and summed in bfloat16 or wider, within the bound.
A program may use at most 128 MiB of HBM per device.

v0:
```python
import jax
import jax.numpy as jnp
from jax import lax
from jax.sharding import Mesh
from jax.sharding import PartitionSpec as P

NOPE_W = 128
V_W = 128
NOPE_N = 64
V_N = 64
ROPE = 64
SP = ("sp_0", "sp_1", "sp_2")
SP_TP = ("sp_0", "sp_1", "sp_2", "tp")


EPS = 1e-06
THETA = 10000.0


def sent_together(arrays, axis, dim, along):
    widths = [a.shape[along] for a in arrays]
    both = jnp.concatenate(arrays, axis=along)
    result = lax.all_gather(both, axis, axis=dim, tiled=True)
    return tuple(jnp.split(result, [sum(widths[:k]) for k in range(1, len(widths))], axis=along))


def in_blocks(array, dim, length):
    lengths = array.shape
    tiles = array.reshape(*lengths[:dim], length, lengths[dim] // length, *lengths[dim + 1 :])
    return jnp.moveaxis(tiles, dim, 0)


def sent_and_summed(array, axis, dim):
    length = lax.axis_size(axis)
    tiles = lax.all_to_all(in_blocks(array, dim, length), axis, 0, 0, tiled=True)
    return jnp.sum(tiles.astype(jnp.float32), axis=0)


def sent_to_all(array, axis):
    copies = jnp.broadcast_to(array, (lax.axis_size(axis), *array.shape))
    return lax.all_to_all(copies, axis, split_axis=0, concat_axis=0, tiled=True)


def in_order(tiles, dim):
    tiles = jnp.moveaxis(tiles, 0, dim)
    lengths = tiles.shape
    return tiles.reshape(*lengths[:dim], lengths[dim] * lengths[dim + 1], *lengths[dim + 2 :])


def collect(array, axis, dim):
    tiles = sent_to_all(array, axis)
    return in_order(tiles, dim)


def moved_by_axis(tiles, axes, order):
    inside = tiles.shape[1:]
    result = tiles.reshape(*(lax.axis_size(a) for a in axes), *inside)
    for k in order:
        result = lax.all_to_all(result, axes[k], k, k, tiled=True)
    return result.reshape(-1, *inside)


def core_and_chips(array, groups, order, split_dim, concat_dim):
    length = lax.axis_size(groups[0]) * lax.axis_size(groups[1])
    tiles = in_blocks(array, split_dim, length)
    return in_order(moved_by_axis(tiles, groups, order), concat_dim)


def rms_scale(values, gain):
    return values * lax.rsqrt(jnp.mean(values * values, axis=-1, keepdims=True) + EPS) * gain


def rotate(values, positions):
    half = values.shape[-1] // 2
    freq = THETA ** (-jnp.arange(half, dtype=jnp.float32) * 2.0 / values.shape[-1])
    angle = positions.astype(jnp.float32)[..., None] * freq
    cosine = jnp.cos(angle)
    sine = jnp.sin(angle)
    real = values.astype(jnp.float32)
    first = real[..., :half]
    second = real[..., half:]
    return jnp.concatenate(
        [first * cosine - second * sine, second * cosine + first * sine], axis=-1
    ).astype(jnp.bfloat16)


def contract(left, right):
    return lax.dot_general(
        left, right, (((1,), (1,)), ((), ())), preferred_element_type=jnp.float32
    )


def attend(carry, q_nope, q_rope, k_nope, k_rope, values, factor):
    top_score, weight_sum, accum = carry
    scores = (contract(q_nope, k_nope) + contract(q_rope, k_rope)) * factor
    new_top = jnp.max(scores, axis=1)
    shrink = jnp.exp(top_score - new_top)
    weights = jnp.exp(scores - new_top[:, None])
    weight_sum = weight_sum * shrink + jnp.sum(weights, axis=1)
    accum = accum * shrink[:, None] + jnp.dot(
        weights.astype(jnp.bfloat16), values, preferred_element_type=jnp.float32
    )
    return (new_top, weight_sum, accum)


def local(
    resid,
    query_wide,
    query_narrow,
    latent,
    rope_key,
    latent_gain,
    key_up_wide,
    value_up_wide,
    key_up_narrow,
    value_up_narrow,
    out_wide,
    out_narrow,
    attn_gain,
    ffn_gain,
    moe_gain,
    routes,
    route_logit,
    expert_gate,
    expert_up,
    expert_down,
):
    tok_rows = latent.shape[0]
    wide_heads = query_wide.shape[1] // (NOPE_W + ROPE)
    narrow_heads = query_narrow.shape[1] // (NOPE_N + ROPE)
    tp_rank = lax.axis_index("tp")
    positions = lax.axis_index(SP) * tok_rows + jnp.arange(tok_rows, dtype=jnp.int32)
    normed = rms_scale(latent.astype(jnp.float32), latent_gain).astype(jnp.bfloat16)
    turned_key = rotate(rope_key, positions)

    def my_columns(weight, count):
        return lax.dynamic_slice_in_dim(weight, tp_rank * count, count, 1)

    mine = (
        my_columns(key_up_wide, wide_heads * NOPE_W),
        my_columns(value_up_wide, wide_heads * V_W),
        my_columns(key_up_narrow, narrow_heads * NOPE_N),
        my_columns(value_up_narrow, narrow_heads * V_N),
    )
    q_wide = query_wide.reshape(tok_rows, wide_heads, NOPE_W + ROPE)
    q_narrow = query_narrow.reshape(tok_rows, narrow_heads, NOPE_N + ROPE)
    wide_turn = rotate(q_wide[:, :, NOPE_W:], positions[:, None])
    narrow_turn = rotate(q_narrow[:, :, NOPE_N:], positions[:, None])
    head_list = []
    number = 0
    head_list.append(
        (
            q_wide[:, number, :NOPE_W],
            wide_turn[:, number],
            0,
            NOPE_W,
            V_W,
            number,
            (NOPE_W + ROPE) ** (-0.5),
        )
    )
    number = 0
    head_list.append(
        (
            q_narrow[:, number, :NOPE_N],
            narrow_turn[:, number],
            2,
            NOPE_N,
            V_N,
            number,
            (NOPE_N + ROPE) ** (-0.5),
        )
    )
    initial = tuple(
        (
            (
                jnp.full((tok_rows,), -jnp.inf, jnp.float32),
                jnp.zeros((tok_rows,), jnp.float32),
                jnp.zeros((tok_rows, head_info[4]), jnp.float32),
            )
            for head_info in head_list
        )
    )
    piece = sent_together((normed, turned_key), SP, 0, 1)
    latent_rows = piece[0]
    key_rows = tuple(
        (
            jnp.dot(latent_rows, weight, preferred_element_type=jnp.float32).astype(jnp.bfloat16)
            for weight in mine
        )
    )
    turned_rows = piece[1]
    updated = []
    for state, head_info in zip(initial, head_list):
        q_nope, q_rope, member, key_width, value_width, number, factor = head_info
        k_nope = key_rows[member]
        values = key_rows[member + 1]
        updated.append(attend(state, q_nope, q_rope, k_nope, turned_rows, values, factor))
    result = tuple(updated)
    head_outs = [
        (accum / weight_sum[:, None]).astype(jnp.bfloat16)
        for top_score, weight_sum, accum in result
    ]
    wide_out = jnp.concatenate(head_outs[:wide_heads], axis=1)
    narrow_out = jnp.concatenate(head_outs[wide_heads:], axis=1)
    row_count = resid.shape[0]
    proj = sent_and_summed(
        (
            jnp.dot(wide_out, out_wide, preferred_element_type=jnp.float32)
            + jnp.dot(narrow_out, out_narrow, preferred_element_type=jnp.float32)
        ).astype(jnp.bfloat16),
        "tp",
        0,
    )
    stream = (resid.astype(jnp.float32) + rms_scale(proj, attn_gain)).astype(jnp.bfloat16)
    moe_in = rms_scale(stream.astype(jnp.float32), ffn_gain).astype(jnp.bfloat16)
    top_count = routes.shape[1]
    experts = lax.axis_size(SP)
    capacity = (3 * row_count * top_count + 2 * experts - 1) // (2 * experts)
    chosen = routes.reshape(-1)
    onehot = (chosen[:, None] == jnp.arange(experts, dtype=jnp.int32)[None, :]).astype(jnp.int32)
    before = jnp.cumsum(onehot, axis=0) - onehot
    slot = jnp.sum(before * onehot, axis=1)
    dest = (chosen * capacity + slot).reshape(row_count, top_count)
    slot_ids = jnp.arange(experts * capacity, dtype=jnp.int32)
    placing = jnp.any(slot_ids[:, None, None] == dest[None, :, :], axis=2).astype(jnp.bfloat16)
    outgoing = jnp.dot(placing, moe_in, preferred_element_type=jnp.float32).astype(jnp.bfloat16)
    outgoing = outgoing.reshape(experts, capacity, moe_in.shape[1])
    gathered = collect(
        lax.all_to_all(outgoing, SP, split_axis=0, concat_axis=0, tiled=True), "tp", 0
    )
    flat = gathered.reshape(-1, gathered.shape[2])
    gate = jnp.dot(flat, expert_gate[0], preferred_element_type=jnp.float32)
    upper = jnp.dot(flat, expert_up[0], preferred_element_type=jnp.float32)
    hidden = (jax.nn.silu(gate) * upper).astype(jnp.bfloat16)
    partial_out = jnp.dot(hidden, expert_down[0], preferred_element_type=jnp.float32).reshape(
        gathered.shape
    )
    summed = sent_and_summed(partial_out.astype(jnp.bfloat16), "tp", 0).astype(jnp.bfloat16)
    returned = core_and_chips(summed, (("sp_0", "sp_1"), "sp_2"), (0, 1), 0, 0)
    flat_back = returned.reshape(experts * capacity, returned.shape[2])
    picked = flat_back[dest]
    share = jax.nn.softmax(route_logit, axis=-1)
    branch = jnp.sum(share[:, :, None] * picked.astype(jnp.float32), axis=1)
    return (stream.astype(jnp.float32) + rms_scale(branch, moe_gain)).astype(jnp.bfloat16)


def solution(mesh):
    split = Mesh(mesh.devices.reshape(8, 4, 2, mesh.shape["tp"]), ("sp_0", "sp_1", "sp_2", "tp"))
    in_specs = (
        P(SP_TP, None),
        P(SP, "tp"),
        P(SP, "tp"),
        P(SP, None),
        P(SP, None),
        P(),
        P(),
        P(),
        P(),
        P(),
        P("tp", None),
        P("tp", None),
        P(),
        P(),
        P(),
        P(SP_TP, None),
        P(SP_TP, None),
        P(SP, None, "tp"),
        P(SP, None, "tp"),
        P(SP, "tp", None),
    )
    out_specs = P(SP_TP, None)
    return jax.shard_map(local, mesh=split, in_specs=in_specs, out_specs=out_specs, check_vma=False)
```

profile of v0, /device:TPU:1, one launch (start us, length us, event | category | flops | bytes accessed | tf_op | source)
XLA Modules:
  0.0 418.1 jit_solution(14353970271405764317)
XLA Ops:
  6.6 0.8 convert_element_type.106
  7.4 0.2 fusion.120
  7.6 0.1 copy.76
  7.7 0.1 copy.77
  7.8 1.0 fusion.73
  8.9 1.0 fusion.75
  9.9 0.8 pad_maximum_fusion
  10.7 1.0 copy.78
  11.7 0.9 slice_convert_fusion
  12.6 0.6 fusion.112
  13.2 91.2 %all-gather.2.cloned.1.call-done = bf16[16384,320]{1,0:T(8,128)(2,1)} async-done(((bf16[256,320]{1,0:T(8,128)(2,1)}), bf16[16384,320]{1,0:T(8,128)(2,1)}) %all-gather.2.cloned.1.call-update) | async-done | bytes 10485776 | tf_op jit(solution)/shard_map/all_gather | solution.py:23
  104.5 14.2 %convolution_bitcast_fusion = f32[256,16384]{0,1:T(8,128)} fusion(bf16[16384,320]{1,0:T(8,128)(2,1)} %all-gather.2.cloned.1.call-done, bf16[256,1,128]{2,0,1:T(8,128)(2,1)} %bitcast.52, bf16[256,256]{1,0:T(8,128)(2,1)} %param.28, s32[]{:T(128)S(6)} %select_n.12), kind=kOutput, calls=%fused_computation.2 | convolution fusion | flops 1074790400 | bytes 25296900 | tf_op jit(solution)/shard_map/dot_general | solution.py:88
  118.7 13.4 %fusion.138 = (f32[256]{0:T(256)S(1)}, f32[256,16384]{0,1:T(8,128)}) fusion(f32[256,16384]{0,1:T(8,128)} %convolution_bitcast_fusion, bf16[16384,320]{1,0:T(8,128)(2,1)} %all-gather.2.cloned.1.call-done, bf16[256,32]{1,0:T(8,128)(2,1)S(1)} %get-tuple-element.10, bf16[256,32]{1,0:T(8,128)(2,1)S(1)} %get-tuple-element.9), kind=kOutput, calls=%fused_computation.139 | convolution fusion | flops 549519104 | bytes 37782528 | tf_op jit(solution)/shard_map/dot_general | solution.py:88
  132.0 8.1 %fusion.4 = f32[256]{0:T(256)S(1)} fusion(f32[256,16384]{0,1:T(8,128)} %get-tuple-element.24, f32[256]{0:T(256)S(1)} %get-tuple-element.23), kind=kLoop, calls=%fused_computation.15 | loop fusion | flops 8388352 | bytes 16779264 | tf_op jit(solution)/shard_map/reduce_sum | solution.py:99
  140.1 10.4 %convolution_bitcast_fusion.1 = f32[256,16384]{0,1:T(8,128)} fusion(bf16[16384,320]{1,0:T(8,128)(2,1)} %all-gather.2.cloned.1.call-done, bf16[256,1,192]{2,0,1:T(8,128)(2,1)S(1)} %bitcast.50, bf16[256,512]{1,0:T(8,128)(2,1)} %param.26, s32[]{:T(128)S(6)} %select_n.11), kind=kOutput, calls=%fused_computation.4 | convolution fusion | flops 2149580800 | bytes 25296900 | tf_op jit(solution)/shard_map/dot_general | solution.py:88
  150.5 12.8 %fusion.137 = (f32[256]{0:T(256)S(1)}, f32[256,16384]{0,1:T(8,128)}) fusion(f32[256,16384]{0,1:T(8,128)} %convolution_bitcast_fusion.1, bf16[16384,320]{1,0:T(8,128)(2,1)} %all-gather.2.cloned.1.call-done, bf16[256,32]{1,0:T(8,128)(2,1)S(1)} %get-tuple-element.15, bf16[256,32]{1,0:T(8,128)(2,1)S(1)} %get-tuple-element.16), kind=kOutput, calls=%fused_computation.138 | convolution fusion | flops 549519104 | bytes 37782528 | tf_op jit(solution)/shard_map/dot_general | solution.py:88
  163.3 8.1 %fusion.2 = f32[256]{0:T(256)S(1)} fusion(f32[256,16384]{0,1:T(8,128)} %get-tuple-element.22, f32[256]{0:T(256)S(1)} %get-tuple-element.21), kind=kLoop, calls=%fused_computation.13 | loop fusion | flops 8388352 | bytes 16779264 | tf_op jit(solution)/shard_map/reduce_sum | solution.py:99
  171.4 11.1 %fusion.64 = bf16[256,128]{1,0:T(8,128)(2,1)S(1)} fusion(bf16[16384,320]{1,0:T(8,128)(2,1)} %all-gather.2.cloned.1.call-done, f32[256,16384]{0,1:T(8,128)} %get-tuple-element.22, f32[256]{0:T(256)S(1)} %get-tuple-element.21, f32[256]{0:T(256)S(1)} %get-tuple-element.20, bf16[256,512]{1,0:T(8,128)(2,1)} %param.27, s32[]{:T(128)S(6)} %select_n.11, ...), kind=kOutput, calls=%fused_computation.45 | convolution fusion | flops 2158067712 | bytes 25299972 | tf_op jit(solution)/shard_map/dot_general | solution.py:100
  182.5 0.4 fusion.139
  183.0 12.2 %fusion.54 = bf16[256,64]{0,1:T(8,128)(2,1)S(1)} fusion(f32[256,16384]{0,1:T(8,128)} %get-tuple-element.24, f32[256]{0:T(256)S(1)} %get-tuple-element.23, bf16[16384,320]{1,0:T(8,128)(2,1)} %all-gather.2.cloned.1.call-done, bf16[256,256]{1,0:T(8,128)(2,1)S(1)} %copy-done.5, s32[]{:T(128)S(6)} %select_n.12, f32[256]{0:T(256)S(1)} %get-tuple-element.18, ...), kind=kOutput, calls=%fused_computation.43 | convolution fusion | flops 1083228160 | bytes 25267204 | tf_op jit(solution)/shard_map/dot_general | solution.py:100
  195.3 1.4 fusion.27
  196.7 4.0 all-to-all-start
  200.7 0.1 copy.82
  200.8 0.1 eq.29
  200.9 0.1 fusion.102
  201.0 0.2 reduce_window_sum.11
  201.2 0.2 select_reduce_fusion
  201.4 0.1 reduce_sum.111
  201.6 0.1 fusion.95
  201.7 13.6 %all-to-all-done = bf16[4,64,2048]{2,1,0:T(8,128)(2,1)S(1)} async-done(((bf16[4,64,2048]{2,1,0:T(8,128)(2,1)}), bf16[4,64,2048]{2,1,0:T(8,128)(2,1)S(1)}, u32[]{:S(2)}, u32[]{:S(2)}) %all-to-all-start) | async-done | bytes 1048608 | tf_op jit(solution)/shard_map/all_to_all | solution.py:35
  215.4 0.2 convert_reduce_fusion
  215.5 0.1 multiply_reduce_fusion.2
  215.7 0.3 fusion.69
  216.0 0.4 convolution_convert_fusion.4
  216.4 0.5 reshape.233
  216.9 35.0 %all_to_all.30 = bf16[64,3,2048]{2,1,0:T(4,128)(2,1)S(1)} all-to-all(bf16[64,3,2048]{2,1,0:T(4,128)(2,1)S(1)} %reshape.233), channel_id=1, replica_groups=mesh['sp_0'=8,'sp_1'=4,'sp_2'=2,'tp'=4] {'sp_0','sp_1','sp_2'}, dimensions={0} | all-to-all | bytes 1572864 | tf_op jit(solution)/shard_map/all_to_all | solution.py:230
  251.9 0.6 copy.84
  252.5 0.4 broadcast_in_dim.7
  252.9 39.2 %all_to_all.31 = bf16[4,64,3,2048]{3,1,2,0:T(8,128)(2,1)S(1)} all-to-all(bf16[4,64,3,2048]{3,1,2,0:T(8,128)(2,1)S(1)} %broadcast_in_dim.7), channel_id=1, replica_groups=mesh['sp_0'=8,'sp_1'=4,'sp_2'=2,'tp'=4] {'tp'}, dimensions={0} | all-to-all | bytes 6291456 | tf_op jit(solution)/shard_map/all_to_all | solution.py:41
  292.1 4.7 %copy.85 = bf16[4,64,3,2048]{3,2,1,0:T(4,128)(2,1)} copy(bf16[4,64,3,2048]{3,1,2,0:T(8,128)(2,1)S(1)} %all_to_all.31) | data formatting | bytes 6291456 | tf_op jit(solution)/shard_map/all_to_all | solution.py:41
  296.8 8.8 %reshape_reshape.6 = bf16[768,2048]{1,0:T(8,128)(2,1)} reshape(bf16[4,64,3,2048]{3,2,1,0:T(4,128)(2,1)} %copy.85) | data formatting | bytes 6291456 | tf_op jit(solution)/shard_map/reshape;reshape | solution.py:232
  305.6 6.5 %fusion.20 = f32[768,896]{1,0:T(8,128)S(1)} fusion(bf16[768,2048]{1,0:T(8,128)(2,1)} %reshape_reshape.6, bf16[1,2048,896]{2,1,0:T(8,128)(2,1)} %param.38), kind=kOutput, calls=%fused_computation.29 | convolution fusion | flops 2818572288 | bytes 9568256 | tf_op jit(solution)/shard_map/dot_general | solution.py:234
  312.2 4.8 %multiply_convert_fusion = bf16[768,896]{1,0:T(8,128)(2,1)} fusion(f32[768,896]{1,0:T(8,128)S(1)} %fusion.20, bf16[768,2048]{1,0:T(8,128)(2,1)S(1)} %copy-done.2, bf16[1,2048,896]{2,1,0:T(8,128)(2,1)S(1)} %copy-done.11), kind=kOutput, calls=%fused_computation.34 | convolution fusion | flops 2822701056 | bytes 10944512 | tf_op jit(solution)/shard_map/dot_general | solution.py:233
  316.9 3.7 dot_general.71
  320.6 5.7 %fusion.24 = bf16[256,3,2048]{2,0,1:T(8,128)(2,1)S(1)} fusion(bf16[1,896,2048]{2,1,0:T(8,128)(2,1)} %param.39, bf16[256,3,896]{2,1,0:T(4,128)(2,1)S(1)} %dot_general.71), kind=kOutput, calls=%fused_computation.33 | convolution fusion | flops 2820145152 | bytes 8192000 | tf_op jit(solution)/shard_map/dot_general | solution.py:236
  326.3 0.4 copy.87
  326.7 38.7 %all_to_all.32 = bf16[4,64,3,2048]{3,1,2,0:T(8,128)(2,1)} all-to-all(bf16[4,64,3,2048]{3,1,2,0:T(8,128)(2,1)S(1)} %copy.87), channel_id=1, replica_groups=mesh['sp_0'=8,'sp_1'=4,'sp_2'=2,'tp'=4] {'tp'}, dimensions={0} | all-to-all | bytes 6291456 | tf_op jit(solution)/shard_map/all_to_all | solution.py:35
  365.4 2.6 reduce_sum.113
  368.0 0.5 reshape_reshape.7
  368.5 1.4 copy.89
  369.9 6.7 %all-to-all-start.4 = ((bf16[32,2,1,3,2048]{4,1,3,2,0:T(2,128)(2,1)}), bf16[32,2,1,3,2048]{4,1,3,2,0:T(2,128)(2,1)S(1)}, u32[]{:S(2)}, u32[]{:S(2)}) async-start(bf16[32,2,1,3,2048]{4,1,3,2,0:T(2,128)(2,1)} %copy.89), calls=%async_computation.4 | async-start | bytes 1572864 | tf_op jit(solution)/shard_map/all_to_all | solution.py:59
  376.6 0.1 copy.92
  376.7 0.1 reshape.237
  376.9 0.1 copy.81
  377.1 19.2 %all-to-all-done.4 = bf16[32,2,1,3,2048]{4,1,3,2,0:T(2,128)(2,1)S(1)} async-done(((bf16[32,2,1,3,2048]{4,1,3,2,0:T(2,128)(2,1)}), bf16[32,2,1,3,2048]{4,1,3,2,0:T(2,128)(2,1)S(1)}, u32[]{:S(2)}, u32[]{:S(2)}) %all-to-all-start.4) | async-done | bytes 786464 | tf_op jit(solution)/shard_map/all_to_all | solution.py:59
  396.3 0.2 copy.90
  396.6 8.9 %all_to_all.33 = bf16[32,2,1,3,2048]{4,0,3,2,1:T(8,128)(2,1)S(1)} all-to-all(bf16[32,2,1,3,2048]{4,0,3,2,1:T(8,128)(2,1)S(1)} %copy.90), channel_id=1, replica_groups=mesh['sp_0'=8,'sp_1'=4,'sp_2'=2,'tp'=4] {'sp_2'}, dimensions={1} | all-to-all | bytes 1572864 | tf_op jit(solution)/shard_map/all_to_all | solution.py:59
  405.4 0.7 copy.91
  406.1 0.7 reshape_reshape_reshape.3
  406.8 0.9 gather_fusion
  407.8 0.7 reshape.245
  408.4 1.5 multiply_reduce_fusion
  410.0 0.1 multiply_reduce_fusion.1
  410.1 0.9 fusion.72
  (40 shorter events, 0.3 us)
Async XLA Ops:
  6.5 176.0 %copy-start = (bf16[128,2048]{1,0:T(8,128)(2,1)S(1)}, bf16[128,2048]{1,0:T(8,128)(2,1)}, u32[]{:S(2)}) copy-start(bf16[128,2048]{1,0:T(8,128)(2,1)} %param.30) | copy-start | bytes 1572868
  6.5 98.0 %all-gather.2.cloned.1.call-start = ((), (), s32[]{:S(2)}) async-start(), calls=%async_computation.6 | async-start | bytes 12779520 | tf_op jit(solution)/shard_map/all_gather | solution.py:23
  171.4 11.5 %copy-start.5 = (bf16[256,256]{1,0:T(8,128)(2,1)S(1)}, bf16[256,256]{1,0:T(8,128)(2,1)}, u32[]{:S(2)}) copy-start(bf16[256,256]{1,0:T(8,128)(2,1)} %param.29) | copy-start | bytes 393220
  183.0 12.3 %copy-start.4 = (bf16[64,2048]{1,0:T(8,128)(2,1)S(1)}, bf16[64,2048]{1,0:T(8,128)(2,1)}, u32[]{:S(2)}) copy-start(bf16[64,2048]{1,0:T(8,128)(2,1)} %param.31) | copy-start | bytes 786436
  183.0 17.7 %copy-start.10 = (s32[64,2]{0,1:T(2,128)S(1)}, s32[64,2]{0,1:T(2,128)}, u32[]{:S(2)}) copy-start(s32[64,2]{0,1:T(2,128)} %param.35) | copy-start | bytes 1540
  195.2 20.4 %copy-start.3 = (bf16[64,2048]{1,0:T(8,128)(2,1)S(1)}, bf16[64,2048]{1,0:T(8,128)(2,1)}, u32[]{:S(2)}) copy-start(bf16[64,2048]{1,0:T(8,128)(2,1)} %param.20) | copy-start | bytes 786436
  195.2 20.4 %copy-start.7 = (f32[2048]{0:T(1024)S(1)}, f32[2048]{0:T(1024)}, u32[]{:S(2)}) copy-start(f32[2048]{0:T(1024)} %param.32) | copy-start | bytes 24580
  195.3 20.7 %copy-start.8 = (f32[2048]{0:T(1024)S(1)}, f32[2048]{0:T(1024)}, u32[]{:S(2)}) copy-start(f32[2048]{0:T(1024)} %param.33) | copy-start | bytes 24580
  196.7 18.7 %all-to-all-start = ((bf16[4,64,2048]{2,1,0:T(8,128)(2,1)}), bf16[4,64,2048]{2,1,0:T(8,128)(2,1)S(1)}, u32[]{:S(2)}, u32[]{:S(2)}) async-start(bf16[4,64,2048]{2,1,0:T(8,128)(2,1)} %bitcast.47), calls=%async_computation | async-start | bytes 2097152 | tf_op jit(solution)/shard_map/all_to_all | solution.py:35
  305.6 6.5 %copy-start.2 = (bf16[768,2048]{1,0:T(8,128)(2,1)S(1)}, bf16[768,2048]{1,0:T(8,128)(2,1)}, u32[]{:S(2)}) copy-start(bf16[768,2048]{1,0:T(8,128)(2,1)} %reshape_reshape.6) | copy-start | bytes 9437188
  305.6 6.5 %copy-start.11 = (bf16[1,2048,896]{2,1,0:T(8,128)(2,1)S(1)}, bf16[1,2048,896]{2,1,0:T(8,128)(2,1)}, u32[]{:S(2)}) copy-start(bf16[1,2048,896]{2,1,0:T(8,128)(2,1)} %param.37) | copy-start | bytes 11010052
  326.7 50.2 %copy-start.6 = (f32[64,2]{0,1:T(2,128)S(1)}, f32[64,2]{0,1:T(2,128)}, u32[]{:S(2)}) copy-start(f32[64,2]{0,1:T(2,128)} %param.36) | copy-start | bytes 1540
  369.9 26.4 %all-to-all-start.4 = ((bf16[32,2,1,3,2048]{4,1,3,2,0:T(2,128)(2,1)}), bf16[32,2,1,3,2048]{4,1,3,2,0:T(2,128)(2,1)S(1)}, u32[]{:S(2)}, u32[]{:S(2)}) async-start(bf16[32,2,1,3,2048]{4,1,3,2,0:T(2,128)(2,1)} %copy.89), calls=%async_computation.4 | async-start | bytes 1572864 | tf_op jit(solution)/shard_map/all_to_all | solution.py:59
  396.5 14.4 %copy-start.1 = (bf16[128,2048]{1,0:T(8,128)(2,1)S(1)}, bf16[128,2048]{1,0:T(8,128)(2,1)}, u32[]{:S(2)}) copy-start(bf16[128,2048]{1,0:T(8,128)(2,1)} %param.30) | copy-start | bytes 1572868
  405.4 4.7 %copy-start.9 = (f32[2048]{0:T(1024)S(1)}, f32[2048]{0:T(1024)}, u32[]{:S(2)}) copy-start(f32[2048]{0:T(1024)} %param.34) | copy-start | bytes 24580
Sparse Core Ops, SparseCore 0:
  10.8 93.6 all-gather.1
where the time goes:
time: 423 us; the launch traced here: 418 us
  waiting for transfers between devices  124 us (29%)
  blocking collectives  122 us (29%)
  matrix products  93.3 us (22%)
  other arithmetic  27.9 us (7%)
  local copies, waits for them, and re-layouts  26.3 us (6%)
  between operations  14 us (3%)
  starting transfers between devices  10.7 us (3%)
    all_gather x1, waiting for transfers between devices, sent_together(): result = lax.all_gather(both, axis, axis=dim, tiled=True)  91.2 us
    dot_general x4, matrix products, contract(): lax.dot_general(left, right, (((1,), (1,)), ((), ())), preferred_element_...  50.7 us
    all_to_all x1, blocking collectives, sent_to_all(): return lax.all_to_all(copies, axis, split_axis=0, concat_axis=0, tiled=True)  39.2 us
    all_to_all x1, blocking collectives, sent_and_summed(): lax.all_to_all(in_blocks(array, dim, length), axis, 0, 0, tiled=True)  38.7 us
    all_to_all x1, blocking collectives, local(): lax.all_to_all(outgoing, SP, split_axis=0, concat_axis=0, tiled=True)  35 us
    dot_general x2, matrix products, attend(): jnp.dot(weights.astype(jnp.bfloat16), values, preferred_element_type=jnp....  23.3 us
    all_to_all x1, waiting for transfers between devices, moved_by_axis(): result = lax.all_to_all(result, axes[k], k, k, tiled=True)  19.2 us
    reduce_sum x2, other arithmetic, attend(): weight_sum = weight_sum * shrink + jnp.sum(weights, axis=1)  16.2 us
  transfers between devices with their start and end apart: 3, of which 3 were waited for; matrix products, arithmetic and copies ran while one was open for 1% of the time, Pallas kernels for 0%

commit v1 on v0

v1 whole, which is shorter than its diff:
```python
import functools
import math

import jax
import jax.numpy as jnp
from jax import lax
from jax.experimental import pallas as pl
from jax.experimental.pallas import tpu as pltpu
from jax.sharding import Mesh
from jax.sharding import PartitionSpec as P

NOPE_W = 128
V_W = 128
NOPE_N = 64
V_N = 64
ROPE = 64
SP = ("sp_0", "sp_1", "sp_2")
SP_TP = ("sp_0", "sp_1", "sp_2", "tp")
NZ, NX, NC, NT = 8, 4, 2, 4
TOK = 256
SUB = 64
LOG2E = math.log2(math.e)
MESH_ID = pl.DeviceIdType.MESH

EPS = 1e-06
THETA = 10000.0


def send(src, dst, send_sem, recv_sem, where):
    copy = pltpu.make_async_remote_copy(
        src_ref=src,
        dst_ref=dst,
        send_sem=send_sem,
        recv_sem=recv_sem,
        device_id=where,
        device_id_type=MESH_ID,
    )
    copy.start()
    return copy


def greet(peers):
    barrier = pltpu.get_barrier_semaphore()
    for peer in peers:
        pl.semaphore_signal(barrier, inc=1, device_id=peer, device_id_type=MESH_ID)
    pl.semaphore_wait(barrier, len(peers))


def mm(a, b):
    return jnp.dot(a, b, preferred_element_type=jnp.float32)


def mm_nt(a, b):
    return lax.dot_general(a, b, (((1,), (1,)), ((), ())), preferred_element_type=jnp.float32)


FACTOR_W = (NOPE_W + ROPE) ** (-0.5) * LOG2E
FACTOR_N = (NOPE_N + ROPE) ** (-0.5) * LOG2E


def attention_kernel(
    q_in,
    kv_in,
    w_in,
    out_ref,
    qbuf,
    kvbuf,
    kw_s,
    kn_s,
    vw_s,
    vn_s,
    top_w,
    top_n,
    acc_w,
    acc_n,
    osend,
    orecv,
    ysend,
    yrecv,
    q_ss,
    q_rs,
    f_ss,
    f_rs,
    b_ss,
    b_rs,
    d_ss,
    d_rs,
    o_ss,
    o_rs,
    y_ss,
    y_rs,
):
    z = lax.axis_index("sp_0")
    x = lax.axis_index("sp_1")
    core = lax.axis_index("sp_2")
    y = lax.axis_index("tp")
    up = {"sp_0": lax.rem(z + 1, NZ)}
    down = {"sp_0": lax.rem(z + NZ - 1, NZ)}
    sibling = {"sp_2": 1 - core}
    xs = {j: {"sp_1": lax.rem(x + j, NX)} for j in range(1, NX)}
    ys = {j: {"tp": lax.rem(y + j, NT)} for j in range(1, NT)}
    greet([up, down, sibling] + list(xs.values()) + list(ys.values()))

    half = TOK // 2

    def piece(r):
        return kv_in if r == 0 else kvbuf.at[r, 0]

    waits = []
    fwd = {1: send(kv_in, kvbuf.at[1, 0], f_ss.at[1], f_rs.at[1], up)}
    bwd = {1: send(kv_in, kvbuf.at[7, 0], b_ss.at[1], b_rs.at[1], down)}
    across = {0: send(kv_in, kvbuf.at[0, 1], d_ss.at[0], d_rs.at[0], sibling)}
    qcopies = {}
    for j in (1, 3, 2):
        qcopies[j] = send(q_in, qbuf.at[j], q_ss.at[j], q_rs.at[j], xs[j])

    lane = lax.broadcasted_iota(jnp.int32, (2 * TOK, 128), 1)
    vw_s[:, 128:] = jnp.ones((2 * TOK, 128), jnp.bfloat16)

    def expand(r):
        w = w_in[...]
        if r == 0:
            kv = jnp.concatenate([kv_in[...], kvbuf[0, 1]], axis=0)
        else:
            kv = kvbuf[r].reshape(2 * TOK, 384)
        full = mm(kv[:, :256], w)
        tail = kv[:, 256:]
        kw_s[:, :128] = full[:, :128].astype(jnp.bfloat16)
        kw_s[:, 128:] = tail
        kn_s[...] = jnp.where(
            lane < 64, full[:, 128:256], tail.astype(jnp.float32)
        ).astype(jnp.bfloat16)
        vw_s[:, :128] = full[:, 256:384].astype(jnp.bfloat16)
        vn_s[...] = jnp.where(lane < 64, full[:, 384:], 1.0).astype(jnp.bfloat16)

    def one_head(q, keys, values, top, acc, j, factor, first):
        scores = mm_nt(q, keys)
        best = jnp.max(scores, axis=1, keepdims=True)
        if not first:
            old = top[j]
            new = jnp.maximum(old, best)
            shrink = jnp.exp2((old - new) * factor)
            best = new[:, :1]
        else:
            new = jnp.broadcast_to(best, (TOK, 128))
        weights = jnp.exp2((scores - best) * factor).astype(jnp.bfloat16)
        summed = mm(weights, values)
        if not first:
            width = summed.shape[1]
            wide = shrink if width == 128 else jnp.concatenate([shrink, shrink], axis=1)
            summed = acc[j] * wide + summed
        acc[j] = summed
        top[j] = new

    def attend(j, q, first):
        one_head(q[:, :256], kw_s[...], vw_s[...], top_w, acc_w, j, FACTOR_W, first)
        one_head(q[:, 256:], kn_s[...], vn_s[...], top_n, acc_n, j, FACTOR_N, first)

    def all_queries(first):
        attend(0, q_in[...], first)

        def body(j, carry):
            attend(j, qbuf[j], first)
            return carry

        lax.fori_loop(1, NX, body, 0)

    across[0].wait_recv()
    expand(0)
    attend(0, q_in[...], True)
    for j in (1, 3, 2):
        qcopies[j].wait_recv()

    def first_body(j, carry):
        attend(j, qbuf[j], True)
        return carry

    lax.fori_loop(1, NX, first_body, 0)

    for k in range(1, 4):
        fwd[k].wait_recv()
        if k < 3:
            fwd[k + 1] = send(
                kvbuf.at[k, 0], kvbuf.at[k + 1, 0], f_ss.at[k + 1], f_rs.at[k + 1], up
            )
        else:
            fwd[4] = send(
                kvbuf.at[3, 0, pl.ds(0, half)],
                kvbuf.at[4, 0, pl.ds(0, half)],
                f_ss.at[4],
                f_rs.at[4],
                up,
            )
        across[k] = send(kvbuf.at[k, 0], kvbuf.at[k, 1], d_ss.at[k], d_rs.at[k], sibling)
        bwd[k].wait_recv()
        if k < 3:
            bwd[k + 1] = send(
                kvbuf.at[8 - k, 0], kvbuf.at[7 - k, 0], b_ss.at[k + 1], b_rs.at[k + 1], down
            )
        else:
            bwd[4] = send(
                kvbuf.at[5, 0, pl.ds(half, half)],
                kvbuf.at[4, 0, pl.ds(half, half)],
                b_ss.at[4],
                b_rs.at[4],
                down,
            )
        across[8 - k] = send(
            kvbuf.at[8 - k, 0], kvbuf.at[8 - k, 1], d_ss.at[8 - k], d_rs.at[8 - k], sibling
        )
        across[k].wait_recv()
        expand(k)
        all_queries(False)
        across[8 - k].wait_recv()
        expand(8 - k)
        all_queries(False)

    fwd[4].wait_recv()
    across[4] = send(
        kvbuf.at[4, 0, pl.ds(0, half)],
        kvbuf.at[4, 1, pl.ds(0, half)],
        d_ss.at[4],
        d_rs.at[4],
        sibling,
    )
    bwd[4].wait_recv()
    across[8] = send(
        kvbuf.at[4, 0, pl.ds(half, half)],
        kvbuf.at[4, 1, pl.ds(half, half)],
        d_ss.at[8],
        d_rs.at[8],
        sibling,
    )
    across[4].wait_recv()
    across[8].wait_recv()
    expand(4)

    lane_q = lax.broadcasted_iota(jnp.int32, (TOK, 128), 1)

    def three(value):
        high = value.astype(jnp.bfloat16).astype(jnp.float32)
        rest = value - high
        middle = rest.astype(jnp.bfloat16).astype(jnp.float32)
        return high, middle, rest - middle

    def finish(j, ref):
        total_w = acc_w[j, :, 128:]
        ref[:, :128] = (acc_w[j, :, :128] / total_w).astype(jnp.bfloat16)
        both = acc_n[j]
        total_n = pltpu.roll(both, 64, 1)
        tail = both / total_n
        level_w = top_w[j] * FACTOR_W + jnp.log2(total_w)
        level_n = top_n[j] * FACTOR_N + jnp.log2(both)
        at = 64
        for part in three(level_w) + three(level_n):
            tail = jnp.where(lane_q == at, part, tail)
            at += 1
        ref[:, 128:] = tail.astype(jnp.bfloat16)

    ocopies = {}
    for j in (2, 1, 3):
        attend(j, qbuf[j], False)
        finish(j, osend.at[j])
        ocopies[j] = send(
            osend.at[j], orecv.at[j], o_ss.at[j], o_rs.at[j], {"sp_1": lax.rem(x + NX - j, NX)}
        )
    attend(0, q_in[...], False)
    finish(0, osend.at[0])
    for j in (1, 3, 2):
        ocopies[j].wait_recv()

    tails = [osend[0, :, 128:].astype(jnp.float32)] + [
        orecv[j, :, 128:].astype(jnp.float32) for j in range(1, NX)
    ]
    mains = [osend[0, :, :128]] + [orecv[j, :, :128] for j in range(1, NX)]

    def shares(at):
        levels = [(t[:, at : at + 1] + t[:, at + 1 : at + 2]) + t[:, at + 2 : at + 3] for t in tails]
        best = functools.reduce(jnp.maximum, levels)
        parts = [jnp.exp2(level - best) for level in levels]
        total = functools.reduce(jnp.add, parts)
        return [part / total for part in parts]

    share_w = shares(64)
    share_n = shares(67)
    merged_w = functools.reduce(
        jnp.add, [m.astype(jnp.float32) * s for m, s in zip(mains, share_w)]
    )
    merged_n = functools.reduce(jnp.add, [t * s for t, s in zip(tails, share_n)])
    ysend[:, :128] = merged_w.astype(jnp.bfloat16)
    ysend[:, 128:] = jnp.where(lane_q < 64, merged_n, 0.0).astype(jnp.bfloat16)
    ycopies = {}
    for j in (2, 1, 3):
        rows = pl.ds(pl.multiple_of(lax.rem(y + j, NT) * SUB, SUB), SUB)
        ycopies[j] = send(ysend.at[rows], yrecv.at[j], y_ss.at[j], y_rs.at[j], ys[j])
    out_ref[0] = ysend[pl.ds(pl.multiple_of(y * SUB, SUB), SUB)]
    for j in range(1, NT):
        ycopies[j].wait_recv()
        out_ref[j] = yrecv[j]
    for group in (fwd, bwd, across, qcopies, ocopies, ycopies):
        for copy in group.values():
            copy.wait_send()


def attention(q, kv, weights):
    bf = jnp.bfloat16
    f32 = jnp.float32
    dma = pltpu.SemaphoreType.DMA
    return pl.pallas_call(
        attention_kernel,
        out_shape=jax.ShapeDtypeStruct((NT, SUB, 256), bf),
        in_specs=[pl.BlockSpec(memory_space=pltpu.VMEM)] * 3,
        out_specs=pl.BlockSpec(memory_space=pltpu.VMEM),
        scratch_shapes=[
            pltpu.VMEM((NX, TOK, 384), bf),
            pltpu.VMEM((NZ, NC, TOK, 384), bf),
            pltpu.VMEM((2 * TOK, 256), bf),
            pltpu.VMEM((2 * TOK, 128), bf),
            pltpu.VMEM((2 * TOK, 256), bf),
            pltpu.VMEM((2 * TOK, 128), bf),
            pltpu.VMEM((NX, TOK, 128), f32),
            pltpu.VMEM((NX, TOK, 128), f32),
            pltpu.VMEM((NX, TOK, 256), f32),
            pltpu.VMEM((NX, TOK, 128), f32),
            pltpu.VMEM((NX, TOK, 256), bf),
            pltpu.VMEM((NX, TOK, 256), bf),
            pltpu.VMEM((TOK, 256), bf),
            pltpu.VMEM((NT, SUB, 256), bf),
            dma((NX,)),
            dma((NX,)),
            dma((5,)),
            dma((5,)),
            dma((5,)),
            dma((5,)),
            dma((9,)),
            dma((9,)),
            dma((NX,)),
            dma((NX,)),
            dma((NT,)),
            dma((NT,)),
        ],
        compiler_params=pltpu.CompilerParams(
            collective_id=0, has_side_effects=True, vmem_limit_bytes=40 * 1024 * 1024
        ),
        cost_estimate=pl.CostEstimate(
            flops=12_000_000_000, bytes_accessed=4_000_000, transcendentals=8_400_000
        ),
        name="attention",
    )(q, kv, weights)


def in_blocks(array, dim, length):
    lengths = array.shape
    tiles = array.reshape(*lengths[:dim], length, lengths[dim] // length, *lengths[dim + 1 :])
    return jnp.moveaxis(tiles, dim, 0)


def sent_and_summed(array, axis, dim):
    length = lax.axis_size(axis)
    tiles = lax.all_to_all(in_blocks(array, dim, length), axis, 0, 0, tiled=True)
    return jnp.sum(tiles.astype(jnp.float32), axis=0)


def sent_to_all(array, axis):
    copies = jnp.broadcast_to(array, (lax.axis_size(axis), *array.shape))
    return lax.all_to_all(copies, axis, split_axis=0, concat_axis=0, tiled=True)


def in_order(tiles, dim):
    tiles = jnp.moveaxis(tiles, 0, dim)
    lengths = tiles.shape
    return tiles.reshape(*lengths[:dim], lengths[dim] * lengths[dim + 1], *lengths[dim + 2 :])


def collect(array, axis, dim):
    tiles = sent_to_all(array, axis)
    return in_order(tiles, dim)


def moved_by_axis(tiles, axes, order):
    inside = tiles.shape[1:]
    result = tiles.reshape(*(lax.axis_size(a) for a in axes), *inside)
    for k in order:
        result = lax.all_to_all(result, axes[k], k, k, tiled=True)
    return result.reshape(-1, *inside)


def core_and_chips(array, groups, order, split_dim, concat_dim):
    length = lax.axis_size(groups[0]) * lax.axis_size(groups[1])
    tiles = in_blocks(array, split_dim, length)
    return in_order(moved_by_axis(tiles, groups, order), concat_dim)


def rms_scale(values, gain):
    return values * lax.rsqrt(jnp.mean(values * values, axis=-1, keepdims=True) + EPS) * gain


def rotate(values, positions):
    half = values.shape[-1] // 2
    freq = THETA ** (-jnp.arange(half, dtype=jnp.float32) * 2.0 / values.shape[-1])
    angle = positions.astype(jnp.float32)[..., None] * freq
    cosine = jnp.cos(angle)
    sine = jnp.sin(angle)
    real = values.astype(jnp.float32)
    first = real[..., :half]
    second = real[..., half:]
    return jnp.concatenate(
        [first * cosine - second * sine, second * cosine + first * sine], axis=-1
    ).astype(jnp.bfloat16)


def local(
    resid,
    query_wide,
    query_narrow,
    latent,
    rope_key,
    latent_gain,
    key_up_wide,
    value_up_wide,
    key_up_narrow,
    value_up_narrow,
    out_wide,
    out_narrow,
    attn_gain,
    ffn_gain,
    moe_gain,
    routes,
    route_logit,
    expert_gate,
    expert_up,
    expert_down,
):
    tp_rank = lax.axis_index("tp")
    out_mine = jnp.concatenate([out_wide, out_narrow], axis=0)
    out_rows = [out_mine] + [
        lax.ppermute(out_mine, "tp", [(i, (i + j) % NT) for i in range(NT)]) for j in range(1, NT)
    ]
    positions = lax.axis_index(SP) * TOK + jnp.arange(TOK, dtype=jnp.int32)
    normed = rms_scale(latent.astype(jnp.float32), latent_gain).astype(jnp.bfloat16)
    turns = rotate(
        jnp.stack([rope_key, query_wide[:, NOPE_W:], query_narrow[:, NOPE_N:]]), positions
    )
    kv = jnp.concatenate([normed, turns[0], turns[0]], axis=1)
    zeros = jnp.zeros((TOK, 64), jnp.bfloat16)
    q = jnp.concatenate(
        [query_wide[:, :NOPE_W], turns[1], zeros, query_narrow[:, :NOPE_N], turns[2]], axis=1
    )

    def my_columns(weight, count):
        mine = lax.dynamic_slice_in_dim(weight, tp_rank * count, count, 1)
        return mine if count == 128 else jnp.concatenate([mine, jnp.zeros_like(mine)], axis=1)

    weights = jnp.concatenate(
        [
            my_columns(key_up_wide, NOPE_W),
            my_columns(key_up_narrow, NOPE_N),
            my_columns(value_up_wide, V_W),
            my_columns(value_up_narrow, V_N),
        ],
        axis=1,
    )
    heads = attention(q, kv, weights)
    proj = jnp.zeros((SUB, 2048), jnp.float32)
    for j in range(NT):
        part = jnp.dot(
            heads[j, :, : V_W + V_N], out_rows[j], preferred_element_type=jnp.float32
        )
        proj = proj + part.astype(jnp.bfloat16).astype(jnp.float32)
    stream = (resid.astype(jnp.float32) + rms_scale(proj, attn_gain)).astype(jnp.bfloat16)
    moe_in = rms_scale(stream.astype(jnp.float32), ffn_gain).astype(jnp.bfloat16)
    row_count = resid.shape[0]
    top_count = routes.shape[1]
    experts = lax.axis_size(SP)
    capacity = (3 * row_count * top_count + 2 * experts - 1) // (2 * experts)
    chosen = routes.reshape(-1)
    onehot = (chosen[:, None] == jnp.arange(experts, dtype=jnp.int32)[None, :]).astype(jnp.int32)
    before = jnp.cumsum(onehot, axis=0) - onehot
    slot = jnp.sum(before * onehot, axis=1)
    dest = (chosen * capacity + slot).reshape(row_count, top_count)
    slot_ids = jnp.arange(experts * capacity, dtype=jnp.int32)
    placing = jnp.any(slot_ids[:, None, None] == dest[None, :, :], axis=2).astype(jnp.bfloat16)
    outgoing = jnp.dot(placing, moe_in, preferred_element_type=jnp.float32).astype(jnp.bfloat16)
    outgoing = outgoing.reshape(experts, capacity, moe_in.shape[1])
    gathered = collect(
        lax.all_to_all(outgoing, SP, split_axis=0, concat_axis=0, tiled=True), "tp", 0
    )
    flat = gathered.reshape(-1, gathered.shape[2])
    gate = jnp.dot(flat, expert_gate[0], preferred_element_type=jnp.float32)
    upper = jnp.dot(flat, expert_up[0], preferred_element_type=jnp.float32)
    hidden = (jax.nn.silu(gate) * upper).astype(jnp.bfloat16)
    partial_out = jnp.dot(hidden, expert_down[0], preferred_element_type=jnp.float32).reshape(
        gathered.shape
    )
    summed = sent_and_summed(partial_out.astype(jnp.bfloat16), "tp", 0).astype(jnp.bfloat16)
    returned = core_and_chips(summed, (("sp_0", "sp_1"), "sp_2"), (0, 1), 0, 0)
    flat_back = returned.reshape(experts * capacity, returned.shape[2])
    picked = flat_back[dest]
    share = jax.nn.softmax(route_logit, axis=-1)
    branch = jnp.sum(share[:, :, None] * picked.astype(jnp.float32), axis=1)
    return (stream.astype(jnp.float32) + rms_scale(branch, moe_gain)).astype(jnp.bfloat16)


def solution(mesh):
    split = Mesh(mesh.devices.reshape(8, 4, 2, mesh.shape["tp"]), ("sp_0", "sp_1", "sp_2", "tp"))
    in_specs = (
        P(SP_TP, None),
        P(SP, "tp"),
        P(SP, "tp"),
        P(SP, None),
        P(SP, None),
        P(),
        P(),
        P(),
        P(),
        P(),
        P("tp", None),
        P("tp", None),
        P(),
        P(),
        P(),
        P(SP_TP, None),
        P(SP_TP, None),
        P(SP, None, "tp"),
        P(SP, None, "tp"),
        P(SP, "tp", None),
    )
    out_specs = P(SP_TP, None)
    return jax.shard_map(local, mesh=split, in_specs=in_specs, out_specs=out_specs, check_vma=False)
```

time: 423 us -> 278 us (0.66)
  waiting for transfers between devices: 124 us -> 19.3 us
  matrix products: 93.3 us -> 18.8 us
  Pallas kernels: 0 us -> 57.8 us
  other arithmetic: 27.9 us -> 7.27 us
  between operations: 14 us -> 0.71 us
  local copies, waits for them, and re-layouts: 26.3 us -> 34 us
    all_gather x1 -> x0, waiting for transfers between devices: 91.2 us -> none  [sent_together(): result = lax.all_gather(both, axis, axis=dim, tiled=True)]
    dot_general x8 -> x4, matrix products: 75.9 us -> 2.27 us  [local(): jnp.dot(heads[j, :, :V_W + V_N], out_rows[j], preferred_element_type=jnp....]
    pallas_call x0 -> x1, Pallas kernels: none -> 57.8 us  [attention(): pl.pallas_call(attention_kernel, out_shape=jax.ShapeDtypeStruct((NT, SUB,...]
    reduce_sum x2 -> x0, other arithmetic: 16.2 us -> none  [attend(): weight_sum = weight_sum * shrink + jnp.sum(weights, axis=1)]
    all_to_all x1 -> x0, waiting for transfers between devices: 13.6 us -> none  [sent_and_summed(): lax.all_to_all(in_blocks(array, dim, length), axis, 0, 0, tiled=True)]
    ppermute x0 -> x3, starting transfers between devices: none -> 5.28 us  [local(): lax.ppermute(out_mine, 'tp', [(i, (i + j) % NT) for i in range(NT)])]
  transfers between devices with their start and end apart: 3 -> 4, of which waited for: 3 -> 1; matrix products, arithmetic and copies ran while one was open for 1% -> 4% of each run, Pallas kernels for 0% -> 21%
where the time goes in v1:
time: 278 us; the launch traced here: 273 us
  blocking collectives  122 us (44%)
  Pallas kernels  57.8 us (21%)
  local copies, waits for them, and re-layouts  34 us (12%)
  waiting for transfers between devices  19.3 us (7%)
  matrix products  18.8 us (7%)
  starting transfers between devices  12.6 us (5%)
  other arithmetic  7.27 us (3%)
    pallas_call x1, Pallas kernels, attention(): pl.pallas_call(attention_kernel, out_shape=jax.ShapeDtypeStruct((NT, SUB,...  57.8 us
    all_to_all x1, blocking collectives, sent_to_all(): return lax.all_to_all(copies, axis, split_axis=0, concat_axis=0, tiled=True)  38.8 us
    all_to_all x1, blocking collectives, sent_and_summed(): lax.all_to_all(in_blocks(array, dim, length), axis, 0, 0, tiled=True)  37.7 us
    all_to_all x1, blocking collectives, local(): lax.all_to_all(outgoing, SP, split_axis=0, concat_axis=0, tiled=True)  37.2 us
    all_to_all x1, waiting for transfers between devices, moved_by_axis(): result = lax.all_to_all(result, axes[k], k, k, tiled=True)  19.3 us
    all_to_all x1, blocking collectives, moved_by_axis(): result = lax.all_to_all(result, axes[k], k, k, tiled=True)  8.4 us
    another operation x1, local copies, waits for them, and re-layouts, local(): flat = gathered.reshape(-1, gathered.shape[2])  7.51 us
    all_to_all x1, starting transfers between devices, moved_by_axis(): result = lax.all_to_all(result, axes[k], k, k, tiled=True)  7.3 us
  transfers between devices with their start and end apart: 4, of which 1 were waited for; matrix products, arithmetic and copies ran while one was open for 4% of the time, Pallas kernels for 21%

profile of v1, /device:TPU:1, one launch (start us, length us, event | category | flops | bytes accessed | tf_op | source)
XLA Modules:
  0.0 272.5 jit_solution(3007427981462388240)
XLA Ops:
  0.0 1.1 constant_dynamic-update-slice_fusion.1
  1.1 1.0 constant_dynamic-update-slice_fusion
  2.1 2.2 collective-permute-start
  4.3 1.5 collective-permute-start.2
  5.8 1.6 collective-permute-start.1
  7.4 0.8 slice.41
  8.1 0.8 slice.40
  9.0 1.0 fusion.46
  10.0 0.1 copy.85
  10.1 0.9 copy.69
  11.0 0.1 copy.84
  11.1 1.0 fusion.23
  12.2 0.8 copy.72
  12.9 0.1 eq.29
  13.1 0.5 multiply_cosine_fusion
  13.7 0.2 add_convert_fusion.1
  13.9 0.1 fusion.34
  14.0 0.1 fusion.25
  14.1 0.1 pad_maximum_fusion.kv_in
  14.2 0.9 constant_dynamic-slice_fusion.1
  15.1 1.0 constant_dynamic-slice_fusion
  16.1 0.1 concatenate.17.q_in
  16.3 0.1 concatenate.19.w_in
  16.5 57.8 %attention.1 = bf16[4,64,256]{2,1,0:T(8,128)(2,1)S(1)} custom-call(bf16[256,384]{1,0:T(8,128)(2,1)S(1)} %concatenate.17.q_in, bf16[256,384]{1,0:T(8,128)(2,1)S(1)} %pad_maximum_fusion.kv_in, bf16[256,512]{1,0:T(8,128)(2,1)S(1)} %concatenate.19.w_in), custom_call_target="tpu_custom_call" | custom-call | flops 12000000000 | bytes 4000000 | tf_op jit(solution)/shard_map/attention/pallas_call | solution.py:309
  74.4 0.2 reduce_window_sum.11
  74.6 0.2 select_reduce_fusion
  74.7 0.1 reduce_sum.81
  75.0 0.1 fusion.29
  75.1 0.3 fusion.15
  75.4 1.4 fusion.9
  76.8 0.3 fusion.14
  77.1 0.4 multiply_reduce_fusion.2
  77.5 0.3 fusion.19
  77.8 0.4 convolution_convert_fusion
  78.2 0.5 reshape.123
  78.7 37.2 %all_to_all.25 = bf16[64,3,2048]{2,1,0:T(4,128)(2,1)S(1)} all-to-all(bf16[64,3,2048]{2,1,0:T(4,128)(2,1)S(1)} %reshape.123), channel_id=1, replica_groups=mesh['sp_0'=8,'sp_1'=4,'sp_2'=2,'tp'=4] {'sp_0','sp_1','sp_2'}, dimensions={0} | all-to-all | bytes 1572864 | tf_op jit(solution)/shard_map/all_to_all | solution.py:486
  115.9 0.6 copy.74
  116.5 0.4 broadcast_in_dim.4
  116.9 38.8 %all_to_all.26 = bf16[4,64,3,2048]{3,1,2,0:T(8,128)(2,1)S(1)} all-to-all(bf16[4,64,3,2048]{3,1,2,0:T(8,128)(2,1)S(1)} %broadcast_in_dim.4), channel_id=1, replica_groups=mesh['sp_0'=8,'sp_1'=4,'sp_2'=2,'tp'=4] {'tp'}, dimensions={0} | all-to-all | bytes 6291456 | tf_op jit(solution)/shard_map/all_to_all | solution.py:366
  155.6 4.7 %copy.75 = bf16[4,64,3,2048]{3,2,1,0:T(4,128)(2,1)} copy(bf16[4,64,3,2048]{3,1,2,0:T(8,128)(2,1)S(1)} %all_to_all.26) | data formatting | bytes 6291456 | tf_op jit(solution)/shard_map/all_to_all | solution.py:366
  160.3 7.5 %reshape_reshape.6 = bf16[768,2048]{1,0:T(8,128)(2,1)S(1)} reshape(bf16[4,64,3,2048]{3,2,1,0:T(4,128)(2,1)} %copy.75) | data formatting | bytes 6291456 | tf_op jit(solution)/shard_map/reshape;reshape | solution.py:488
  167.8 5.6 %fusion.2 = f32[768,896]{1,0:T(8,128)S(1)} fusion(bf16[768,2048]{1,0:T(8,128)(2,1)S(1)} %reshape_reshape.6, bf16[1,2048,896]{2,1,0:T(8,128)(2,1)} %param.38), kind=kOutput, calls=%fused_computation.3 | convolution fusion | flops 2818572288 | bytes 9568256 | tf_op jit(solution)/shard_map/dot_general | solution.py:490
  173.4 4.8 %multiply_convert_fusion = bf16[768,896]{1,0:T(8,128)(2,1)} fusion(f32[768,896]{1,0:T(8,128)S(1)} %fusion.2, bf16[768,2048]{1,0:T(8,128)(2,1)S(1)} %reshape_reshape.6, bf16[1,2048,896]{2,1,0:T(8,128)(2,1)S(1)} %copy-done.8), kind=kOutput, calls=%fused_computation.8 | convolution fusion | flops 2822701056 | bytes 10944512 | tf_op jit(solution)/shard_map/dot_general | solution.py:489
  178.2 3.7 %dot_general.33 = bf16[256,3,896]{2,1,0:T(4,128)(2,1)S(1)} reshape(bf16[768,896]{1,0:T(8,128)(2,1)} %multiply_convert_fusion) | data formatting | bytes 2752512 | tf_op jit(solution)/shard_map/dot_general | solution.py:492
  182.0 5.7 %fusion.6 = bf16[256,3,2048]{2,0,1:T(8,128)(2,1)S(1)} fusion(bf16[1,896,2048]{2,1,0:T(8,128)(2,1)} %param.39, bf16[256,3,896]{2,1,0:T(4,128)(2,1)S(1)} %dot_general.33), kind=kOutput, calls=%fused_computation.7 | convolution fusion | flops 2820145152 | bytes 8192000 | tf_op jit(solution)/shard_map/dot_general | solution.py:492
  187.6 0.4 copy.77
  188.1 37.7 %all_to_all.27 = bf16[4,64,3,2048]{3,1,2,0:T(8,128)(2,1)S(1)} all-to-all(bf16[4,64,3,2048]{3,1,2,0:T(8,128)(2,1)S(1)} %copy.77), channel_id=1, replica_groups=mesh['sp_0'=8,'sp_1'=4,'sp_2'=2,'tp'=4] {'tp'}, dimensions={0} | all-to-all | bytes 6291456 | tf_op jit(solution)/shard_map/all_to_all | solution.py:360
  225.8 1.7 reduce_sum.83
  227.4 2.2 reshape_reshape.7
  229.6 1.4 copy.79
  231.0 7.3 %all-to-all-start.3 = ((bf16[32,2,1,3,2048]{4,1,3,2,0:T(2,128)(2,1)}), bf16[32,2,1,3,2048]{4,1,3,2,0:T(2,128)(2,1)S(1)}, u32[]{:S(2)}, u32[]{:S(2)}) async-start(bf16[32,2,1,3,2048]{4,1,3,2,0:T(2,128)(2,1)} %copy.79), calls=%async_computation.3 | async-start | bytes 1572864 | tf_op jit(solution)/shard_map/all_to_all | solution.py:384
  238.3 0.1 copy.82
  238.4 0.1 reshape.127
  238.6 0.1 copy.71
  238.8 19.3 %all-to-all-done.3 = bf16[32,2,1,3,2048]{4,1,3,2,0:T(2,128)(2,1)S(1)} async-done(((bf16[32,2,1,3,2048]{4,1,3,2,0:T(2,128)(2,1)}), bf16[32,2,1,3,2048]{4,1,3,2,0:T(2,128)(2,1)S(1)}, u32[]{:S(2)}, u32[]{:S(2)}) %all-to-all-start.3) | async-done | bytes 786464 | tf_op jit(solution)/shard_map/all_to_all | solution.py:384
  258.1 0.2 copy.80
  258.3 8.4 %all_to_all.28 = bf16[32,2,1,3,2048]{4,0,3,2,1:T(8,128)(2,1)S(1)} all-to-all(bf16[32,2,1,3,2048]{4,0,3,2,1:T(8,128)(2,1)S(1)} %copy.80), channel_id=1, replica_groups=mesh['sp_0'=8,'sp_1'=4,'sp_2'=2,'tp'=4] {'sp_2'}, dimensions={1} | all-to-all | bytes 1572864 | tf_op jit(solution)/shard_map/all_to_all | solution.py:384
  266.7 0.7 copy.81
  267.4 0.7 reshape_reshape_reshape.3
  268.1 0.9 gather_fusion
  269.1 0.7 reshape.135
  269.7 1.5 multiply_reduce_fusion
  271.3 0.1 multiply_reduce_fusion.1
  271.4 0.9 fusion.22
  (36 shorter events, 0.4 us)
Async XLA Ops:
  0.0 14.0 %copy-start = (bf16[256,256]{1,0:T(8,128)(2,1)S(1)}, bf16[256,256]{1,0:T(8,128)(2,1)}, u32[]{:S(2)}) copy-start(bf16[256,256]{1,0:T(8,128)(2,1)} %param.23) | copy-start | bytes 393220
  0.0 14.0 %copy-start.7 = (f32[256]{0:T(256)S(1)}, f32[256]{0:T(256)}, u32[]{:S(2)}) copy-start(f32[256]{0:T(256)} %param.25) | copy-start | bytes 3076
  2.1 74.7 %collective-permute-start = (bf16[192,2048]{1,0:T(8,128)(2,1)S(1)}, bf16[192,2048]{1,0:T(8,128)(2,1)S(1)}, u32[]{:S(2)}, u32[]{:S(2)}) collective-permute-start(bf16[192,2048]{1,0:T(8,128)(2,1)S(1)} %constant_dynamic-update-slice_fusion), channel_id=1, source_target_pairs={{0,1},{1,2},{2,3},{3,0},{4,5},{5,6},{6,7},{7,4},{8,9},{9,10},{10,1... | collective-permute-start | bytes 2359304 | tf_op jit(solution)/shard_map/ppermute | solution.py:437
  4.3 71.1 %collective-permute-start.2 = (bf16[192,2048]{1,0:T(8,128)(2,1)S(1)}, bf16[192,2048]{1,0:T(8,128)(2,1)}, u32[]{:S(2)}, u32[]{:S(2)}) collective-permute-start(bf16[192,2048]{1,0:T(8,128)(2,1)S(1)} %constant_dynamic-update-slice_fusion), channel_id=1, source_target_pairs={{0,3},{1,0},{2,1},{3,2},{4,7},{5,4},{6,5},{7,6},{8,11},{9,8},{10,9... | collective-permute-start | bytes 2359304 | tf_op jit(solution)/shard_map/ppermute | solution.py:437
  5.8 71.2 %collective-permute-start.1 = (bf16[192,2048]{1,0:T(8,128)(2,1)S(1)}, bf16[192,2048]{1,0:T(8,128)(2,1)S(1)}, u32[]{:S(2)}, u32[]{:S(2)}) collective-permute-start(bf16[192,2048]{1,0:T(8,128)(2,1)S(1)} %constant_dynamic-update-slice_fusion), channel_id=1, source_target_pairs={{0,2},{1,3},{2,0},{3,1},{4,6},{5,7},{6,4},{7,5},{8,10},{9,11},{10,... | collective-permute-start | bytes 2359304 | tf_op jit(solution)/shard_map/ppermute | solution.py:437
  16.4 58.5 %copy-start.6 = (s32[64,2]{0,1:T(2,128)S(1)}, s32[64,2]{0,1:T(2,128)}, u32[]{:S(2)}) copy-start(s32[64,2]{0,1:T(2,128)} %param.35) | copy-start | bytes 1540
  75.1 2.4 copy-start.1
  75.1 2.4 copy-start.3
  75.4 2.4 copy-start.4
  167.8 5.6 %copy-start.8 = (bf16[1,2048,896]{2,1,0:T(8,128)(2,1)S(1)}, bf16[1,2048,896]{2,1,0:T(8,128)(2,1)}, u32[]{:S(2)}) copy-start(bf16[1,2048,896]{2,1,0:T(8,128)(2,1)} %param.37) | copy-start | bytes 11010052
  227.4 11.1 %copy-start.2 = (f32[64,2]{0,1:T(2,128)S(1)}, f32[64,2]{0,1:T(2,128)}, u32[]{:S(2)}) copy-start(f32[64,2]{0,1:T(2,128)} %param.36) | copy-start | bytes 1540
  231.0 27.0 %all-to-all-start.3 = ((bf16[32,2,1,3,2048]{4,1,3,2,0:T(2,128)(2,1)}), bf16[32,2,1,3,2048]{4,1,3,2,0:T(2,128)(2,1)S(1)}, u32[]{:S(2)}, u32[]{:S(2)}) async-start(bf16[32,2,1,3,2048]{4,1,3,2,0:T(2,128)(2,1)} %copy.79), calls=%async_computation.3 | async-start | bytes 1572864 | tf_op jit(solution)/shard_map/all_to_all | solution.py:384
  268.1 3.3 %copy-start.5 = (f32[2048]{0:T(1024)S(1)}, f32[2048]{0:T(1024)}, u32[]{:S(2)}) copy-start(f32[2048]{0:T(1024)} %param.34) | copy-start | bytes 24580

commit v2 on v0

v2 whole, which is shorter than its diff:
```python
import functools
import math

import jax
import jax.numpy as jnp
from jax import lax
from jax.experimental import pallas as pl
from jax.experimental.pallas import tpu as pltpu
from jax.sharding import Mesh
from jax.sharding import PartitionSpec as P

NOPE_W = 128
NOPE_N = 64
ROPE = 64
SP = ("sp_0", "sp_1", "sp_2")
SP_TP = ("sp_0", "sp_1", "sp_2", "tp")
NZ, NX, NC, NT = 8, 4, 2, 4
TOK = 256
SUB = 64
D = 2048
LOG2E = math.log2(math.e)
MESH_ID = pl.DeviceIdType.MESH

EPS = 1e-06
THETA = 10000.0

GROUP = NX * NC
SLOTS = 3
PARTS = 2
LANES = D // PARTS
CHUNKS = SLOTS * PARTS
ROWS = NZ * GROUP
HID = 896
HALF = ROWS // 2

FACTOR_W = (NOPE_W + ROPE) ** (-0.5) * LOG2E
FACTOR_N = (NOPE_N + ROPE) ** (-0.5) * LOG2E

BF = jnp.bfloat16
F32 = jnp.float32

SLOT_OF = {0: 0, 1: 1, 7: 2, 2: 3, 6: 4, 3: 5, 5: 6, 4: 7}


def plan(src, dst, send_sem, recv_sem, where):
    return pltpu.make_async_remote_copy(
        src_ref=src,
        dst_ref=dst,
        send_sem=send_sem,
        recv_sem=recv_sem,
        device_id=where,
        device_id_type=MESH_ID,
    )


def send(*args):
    copy = plan(*args)
    copy.start()
    return copy


def mm(a, b):
    return jnp.dot(a, b, preferred_element_type=F32)


def mm_nt(a, b):
    return lax.dot_general(a, b, (((1,), (1,)), ((), ())), preferred_element_type=F32)


def rms_scale(values, gain):
    return values * lax.rsqrt(jnp.mean(values * values, axis=-1, keepdims=True) + EPS) * gain


def events():
    out = []
    z_step, y_step = 7.0 / PARTS, 8.4 / PARTS
    for c in range(CHUNKS):
        at_z = 3 + z_step * (c + 1)
        at_x = at_z + 4
        near = max(at_x + 5, 10.5 + 4 + y_step * c)
        out.append((at_z, 0, "z", c))
        out.append((at_x, 1, "x", c))
        out.append((near, 2, "near", c))
        out.append((near + 3.5, 3, "gate", c))
    last = 0.0
    for s in range(SLOTS):
        ready = max(at for at, _, name, c in out if name == "gate" and c == s * PARTS + PARTS - 1)
        out.append((ready + 0.1, 4, "act", s))
        for h in range(PARTS):
            c = s * PARTS + h
            down = ready + 0.2 + 0.01 * h
            join = max(down + 5, last + y_step)
            done = join + 4
            last = join
            out.append((down, 5, "down", c))
            out.append((join, 6, "join", c))
            out.append((done, 7, "sum", c))
            out.append((done + 4, 8, "back", c))
            out.append((done + 10, 9, "pick", c))
    return [(name, c) for _, _, name, c in sorted(out)]


def layer_kernel(
    latent,
    latent_gain,
    rope_t,
    wide_t,
    narrow_t,
    cosine,
    sine,
    key_wide,
    value_wide,
    key_narrow,
    value_narrow,
    resid,
    attn_gain,
    ffn_gain,
    routes_t,
    logit_t,
    out_wide,
    out_narrow,
    gate_hbm,
    up_hbm,
    down_hbm,
    branch_ref,
    stream_ref,
    qbuf,
    kvbuf,
    w_kv,
    kw_s,
    kn_s,
    vw_s,
    vn_s,
    top_w,
    top_n,
    acc_w,
    acc_n,
    osend,
    orecv,
    ysend,
    yrecv,
    wbuf,
    moe_in,
    sbuf,
    zbuf,
    xsend,
    rows,
    w_in,
    w_out,
    accum,
    hidden,
    pbuf,
    relay,
    ring,
    ebuf,
    xback,
    zsend,
    zback,
    l_sem,
    q_ss,
    q_rs,
    f_ss,
    f_rs,
    b_ss,
    b_rs,
    d_ss,
    d_rs,
    o_ss,
    o_rs,
    h_ss,
    h_rs,
    w_ss,
    w_rs,
    zl_sem,
    z_ss,
    z_rs,
    xl_sem,
    x_ss,
    x_rs,
    y_ss,
    y_rs,
    r_ss,
    r_rs,
    bl_sem,
    bx_ss,
    bx_rs,
    cl_sem,
    bz_ss,
    bz_rs,
):
    z = lax.axis_index("sp_0")
    x = lax.axis_index("sp_1")
    core = lax.axis_index("sp_2")
    y = lax.axis_index("tp")
    zs = {d: lax.rem(z + d, NZ) for d in range(1, NZ)}
    gs = {}
    for dx in range(NX):
        for dc in range(NC):
            if dx or dc:
                gs[dx * NC + dc] = (lax.rem(x + dx, NX), lax.rem(core + dc, NC))
    xs = {j: {"sp_1": lax.rem(x + j, NX)} for j in range(1, NX)}
    ys = {j: {"tp": lax.rem(y + j, NT)} for j in range(1, NT)}
    up, down = {"sp_0": zs[1]}, {"sp_0": zs[7]}
    right, left = ys[1], ys[3]
    sibling = {"sp_2": 1 - core}
    mine = x * NC + core

    peers = [{"sp_0": p} for p in zs.values()]
    peers += [{"sp_1": a, "sp_2": b} for a, b in gs.values()]
    peers += list(ys.values())
    barrier = pltpu.get_barrier_semaphore()
    for peer in peers:
        pl.semaphore_signal(barrier, inc=1, device_id=peer, device_id_type=MESH_ID)

    loads = [
        pltpu.make_async_copy(out_wide, wbuf.at[0, pl.ds(0, 128)], l_sem.at[0]),
        pltpu.make_async_copy(out_narrow, wbuf.at[0, pl.ds(128, 64)], l_sem.at[1]),
        pltpu.make_async_copy(gate_hbm.at[0], w_in.at[:, pl.ds(0, HID)], l_sem.at[2]),
        pltpu.make_async_copy(up_hbm.at[0], w_in.at[:, pl.ds(HID, HID)], l_sem.at[3]),
        pltpu.make_async_copy(down_hbm.at[0], w_out, l_sem.at[4]),
    ]
    for load in loads:
        load.start()

    def turn(values):
        first, second = values[:32].astype(F32), values[32:].astype(F32)
        c, s = cosine[...], sine[...]
        return jnp.concatenate([first * c - second * s, second * c + first * s], axis=0)

    kvbuf[0, 0, :TOK] = rms_scale(latent[...].astype(F32), latent_gain[...]).astype(BF)
    kvbuf[0, 0, TOK:] = turn(rope_t[...]).astype(BF)
    qbuf[0, :, :128] = wide_t[:128].astype(F32).T.astype(BF)
    qbuf[0, :, 128:256] = (
        jnp.concatenate([turn(wide_t[128:]), jnp.zeros((64, TOK), F32)], axis=0).T.astype(BF)
    )
    qbuf[0, :, 256:] = (
        jnp.concatenate([narrow_t[:64].astype(F32), turn(narrow_t[64:])], axis=0).T.astype(BF)
    )

    pl.semaphore_wait(barrier, len(peers))

    half = 160
    fwd, bwd, across = {}, {}, {}

    def at(r):
        return SLOT_OF[r % NZ]

    for k in range(1, 4):
        fwd[k] = plan(
            kvbuf.at[at(k - 1), 0], kvbuf.at[at(k), 0], f_ss.at[k], f_rs.at[k], up
        )
        bwd[k] = plan(
            kvbuf.at[at(1 - k), 0], kvbuf.at[at(-k), 0], b_ss.at[k], b_rs.at[k], down
        )
    first, second = pl.ds(0, half), pl.ds(half, half)
    fwd[4] = plan(
        kvbuf.at[at(3), 0, first], kvbuf.at[at(4), 0, first], f_ss.at[4], f_rs.at[4], up
    )
    bwd[4] = plan(
        kvbuf.at[at(5), 0, second], kvbuf.at[at(4), 0, second], b_ss.at[4], b_rs.at[4], down
    )
    for r in (0, 1, 2, 3, 5, 6, 7):
        across[r] = plan(
            kvbuf.at[at(r), 0], kvbuf.at[at(r), 1], d_ss.at[r], d_rs.at[r], sibling
        )
    across[4] = plan(
        kvbuf.at[at(4), 0, first], kvbuf.at[at(4), 1, first], d_ss.at[4], d_rs.at[4], sibling
    )
    across[8] = plan(
        kvbuf.at[at(4), 0, second], kvbuf.at[at(4), 1, second], d_ss.at[8], d_rs.at[8], sibling
    )
    fwd[1].start()
    bwd[1].start()
    across[0].start()
    qcopies = {
        j: send(qbuf.at[0], qbuf.at[j], q_ss.at[j], q_rs.at[j], xs[j]) for j in (1, 3, 2)
    }
    upper, lower = pl.ds(0, 96), pl.ds(96, 96)
    wcopies = [
        plan(wbuf.at[0], wbuf.at[1], w_ss.at[0], w_rs.at[0], right),
        plan(wbuf.at[0], wbuf.at[3], w_ss.at[1], w_rs.at[1], left),
        plan(wbuf.at[1, upper], wbuf.at[2, upper], w_ss.at[2], w_rs.at[2], right),
        plan(wbuf.at[3, lower], wbuf.at[2, lower], w_ss.at[3], w_rs.at[3], left),
    ]
    loads[0].wait()
    loads[1].wait()
    wcopies[0].start()
    wcopies[1].start()

    lane_w = lax.broadcasted_iota(jnp.int32, (256, 128), 1)
    wide_at = pl.ds(pl.multiple_of(y * 128, 128), 128)
    narrow_at = pl.ds(pl.multiple_of(y // 2 * 128, 128), 128)
    odd = lax.rem(y, 2) == 1

    def narrow(ref):
        both = ref[:, narrow_at].astype(F32)
        return jnp.where(lane_w < 64, jnp.where(odd, pltpu.roll(both, 64, 1), both), 0.0)

    w_kv[:, :128] = key_wide[:, wide_at]
    w_kv[:, 128:256] = narrow(key_narrow).astype(BF)
    w_kv[:, 256:384] = value_wide[:, wide_at]
    w_kv[:, 384:] = narrow(value_narrow).astype(BF)
    vw_s[:, 128:] = jnp.ones((6 * TOK, 128), BF)

    expert = lax.broadcasted_iota(jnp.int32, (SUB, SUB), 0)
    lane = lax.broadcasted_iota(jnp.int32, (SUB, SUB), 1)
    diagonal = expert == lane

    def column(row):
        return jnp.sum(jnp.where(diagonal, row, 0.0), axis=1, keepdims=True)

    chosen = [routes_t[k : k + 1, :] for k in range(2)]
    named = [(expert == row).astype(F32) for row in chosen]
    earlier = (expert < lane).astype(BF)
    before = mm((named[0] + named[1]).astype(BF), earlier)
    slots = [jnp.sum(before * one, axis=0, keepdims=True) for one in named]
    named_here = [(column(row.astype(F32)) == lane.astype(F32)) for row in chosen]
    slots_here = [column(row) for row in slots]

    def placing(s):
        return jnp.where(slots[0] == s, named[0], 0.0) + jnp.where(slots[1] == s, named[1], 0.0)

    def picking(k, s):
        return jnp.where(named_here[k] & (slots_here[k] == s), 1.0, 0.0).astype(BF)

    logits = [logit_t[k : k + 1, :] for k in range(2)]
    peak = jnp.maximum(logits[0], logits[1])
    parts = [jnp.exp(row - peak) for row in logits]
    share = [column(part / (parts[0] + parts[1])) for part in parts]
    order = (expert // NZ == lax.rem(lane, GROUP)) & (lax.rem(expert, NZ) == lane // GROUP)
    order_back = (expert // GROUP == lax.rem(lane, NZ)) & (lax.rem(expert, GROUP) == lane // NZ)
    order = order.astype(F32).astype(BF)
    order_back = order_back.astype(F32).astype(BF)

    lane_q = lax.broadcasted_iota(jnp.int32, (TOK, 128), 1)

    def expand(base, count):
        def one(i, carry):
            piece = kvbuf[base + i // NC, lax.rem(i, NC)]
            to = pl.ds(pl.multiple_of(i * TOK, TOK), TOK)
            full = mm(piece[:TOK], w_kv[...])
            turned = piece[TOK:].astype(F32)
            tail = jnp.concatenate([turned, turned], axis=0).T
            kw_s[to, :128] = full[:, :128].astype(BF)
            kw_s[to, 128:] = tail.astype(BF)
            kn_s[to] = jnp.where(lane_q < 64, full[:, 128:256], tail).astype(BF)
            vw_s[to, :128] = full[:, 256:384].astype(BF)
            vn_s[to] = jnp.where(lane_q < 64, full[:, 384:], 1.0).astype(BF)
            return carry

        lax.fori_loop(0, count * NC, one, 0)

    def one_head(q, keys, values, top, acc, j, factor, fresh):
        scores = mm_nt(q, keys)
        best = jnp.max(scores, axis=1, keepdims=True)
        if fresh:
            new = jnp.broadcast_to(best, (TOK, 128))
        else:
            old = top[j]
            new = jnp.maximum(old, best)
            shrink = jnp.exp2((old - new) * factor)
            best = new[:, :1]
        weights = jnp.exp2((scores - best) * factor).astype(BF)
        summed = mm(weights, values)
        if not fresh:
            wide = shrink if summed.shape[1] == 128 else jnp.concatenate([shrink, shrink], axis=1)
            summed = acc[j] * wide + summed
        acc[j] = summed
        top[j] = new

    def attend(j, count, fresh):
        keys = count * NC * TOK
        q = qbuf[j]
        one_head(q[:, :256], kw_s[:keys], vw_s[:keys], top_w, acc_w, j, FACTOR_W, fresh)
        one_head(q[:, 256:], kn_s[:keys], vn_s[:keys], top_n, acc_n, j, FACTOR_N, fresh)

    def forward(k):
        fwd[k].wait_recv()
        fwd[k + 1].start()
        across[k].start()
        bwd[k].wait_recv()
        bwd[k + 1].start()
        across[NZ - k].start()

    forward(1)
    for r in (0, 1, 7):
        across[r].wait_recv()
    expand(0, 3)

    def first_body(j, carry):
        for other in range(1, NX):

            @pl.when(j == other)
            def _():
                qcopies[other].wait_recv()

        attend(j, 3, True)

        @pl.when(j == 1)
        def _():
            forward(2)

        return carry

    lax.fori_loop(0, NX, first_body, 0)
    for r in (2, 6):
        across[r].wait_recv()
    expand(3, 2)

    def second_body(j, carry):
        attend(j, 2, False)

        @pl.when(j == 1)
        def _():
            forward(3)
            wcopies[0].wait_recv()
            wcopies[2].start()
            wcopies[1].wait_recv()
            wcopies[3].start()

        return carry

    lax.fori_loop(0, NX, second_body, 0)
    fwd[4].wait_recv()
    across[4].start()
    bwd[4].wait_recv()
    across[8].start()
    for r in (3, 5, 4, 8):
        across[r].wait_recv()
    expand(5, 3)

    def three(value):
        high = value.astype(BF).astype(F32)
        rest = value - high
        middle = rest.astype(BF).astype(F32)
        return high, middle, rest - middle

    def finish(j):
        total_w = acc_w[j, :, 128:]
        osend[j, :, :128] = (acc_w[j, :, :128] / total_w).astype(BF)
        both = acc_n[j]
        tail = both / pltpu.roll(both, 64, 1)
        level_w = top_w[j] * FACTOR_W + jnp.log2(total_w)
        level_n = top_n[j] * FACTOR_N + jnp.log2(both)
        at_lane = 64
        for part in three(level_w) + three(level_n):
            tail = jnp.where(lane_q == at_lane, part, tail)
            at_lane += 1
        osend[j, :, 128:] = tail.astype(BF)

    ocopies = {
        j: plan(osend.at[j], orecv.at[j], o_ss.at[j], o_rs.at[j], xs[NX - j]) for j in (1, 2, 3)
    }

    def last_body(i, carry):
        j = NX - 1 - i
        attend(j, 3, False)
        finish(j)
        for other in range(1, NX):

            @pl.when(j == other)
            def _():
                ocopies[other].start()

        return carry

    lax.fori_loop(0, NX, last_body, 0)
    for j in (3, 2, 1):
        ocopies[j].wait_recv()

    tails = [osend[0, :, 128:].astype(F32)] + [orecv[j, :, 128:].astype(F32) for j in (1, 2, 3)]
    mains = [osend[0, :, :128]] + [orecv[j, :, :128] for j in (1, 2, 3)]

    def weigh(a):
        levels = [(t[:, a : a + 1] + t[:, a + 1 : a + 2]) + t[:, a + 2 : a + 3] for t in tails]
        best = functools.reduce(jnp.maximum, levels)
        portions = [jnp.exp2(level - best) for level in levels]
        total = functools.reduce(jnp.add, portions)
        return [portion / total for portion in portions]

    merged_w = functools.reduce(jnp.add, [m.astype(F32) * s for m, s in zip(mains, weigh(64))])
    merged_n = functools.reduce(jnp.add, [t * s for t, s in zip(tails, weigh(67))])
    ysend[:, :128] = merged_w.astype(BF)
    ysend[:, 128:] = jnp.where(lane_q < 64, merged_n, 0.0).astype(BF)
    hcopies = {}
    for j in (2, 1, 3):
        part = pl.ds(pl.multiple_of(lax.rem(y + j, NT) * SUB, SUB), SUB)
        hcopies[j] = send(ysend.at[part], yrecv.at[j], h_ss.at[j], h_rs.at[j], ys[j])

    own = ysend[pl.ds(pl.multiple_of(y * SUB, SUB), SUB)]
    proj = mm(own[:, :192], wbuf[0]).astype(BF).astype(F32)
    for j, needed in ((1, (0,)), (3, (1,)), (2, (2, 3))):
        if j == 2:
            for copy in needed:
                wcopies[copy].wait_recv()
        hcopies[j].wait_recv()
        proj = proj + mm(yrecv[j, :, :192], wbuf[j]).astype(BF).astype(F32)
    stream = (resid[...].astype(F32) + rms_scale(proj, attn_gain[...])).astype(BF)
    stream_ref[...] = stream
    moe_in[...] = rms_scale(stream.astype(F32), ffn_gain[...]).astype(BF)

    z_order = (4, 3, 5, 2, 6, 1, 7)
    x_order = (4, 5, 2, 3, 6, 7, 1)

    def seg(number):
        return pl.ds(pl.multiple_of(number * 8, 8), 8)

    def over_z(src, dst, c, local_sem, ss, rs):
        copies = {
            d: send(
                src.at[c, seg(zs[d])],
                dst.at[c, seg(z)],
                ss.at[c, d],
                rs.at[c, d],
                {"sp_0": zs[d]},
            )
            for d in z_order
        }
        kept = pltpu.make_async_copy(src.at[c, seg(z)], dst.at[c, seg(z)], local_sem.at[c])
        kept.start()
        return copies, kept

    def over_x(src, dst, c, local_sem, ss, rs):
        copies = {}
        for d in x_order:
            a, b = gs[d]
            copies[d] = send(
                src(c, seg(a * NC + b)),
                dst(c, seg(mine)),
                ss.at[c, d],
                rs.at[c, d],
                {"sp_1": a, "sp_2": b},
            )
        kept = pltpu.make_async_copy(src(c, seg(mine)), dst(c, seg(mine)), local_sem.at[c])
        kept.start()
        return copies, kept

    def arrived(moved):
        copies, kept = moved
        kept.wait()
        for copy in copies.values():
            copy.wait_recv()

    def lanes(c):
        h = c % PARTS
        return slice(h * LANES, (h + 1) * LANES)

    z_moves, x_moves, near, far = {}, {}, {}, {}
    sums, joined, back_x, back_z = {}, {}, {}, {}
    high, low = pl.ds(0, HALF), pl.ds(HALF, HALF)

    for s in range(SLOTS):
        place = placing(s).astype(BF)
        for h in range(PARTS):
            c = s * PARTS + h
            sbuf[c] = mm(place, moe_in[:, lanes(c)]).astype(BF)
            z_moves[c] = over_z(sbuf, zbuf, c, zl_sem, z_ss, z_rs)

    def stage_z(c):
        arrived(z_moves[c])
        xsend[c] = mm(order, zbuf[c]).astype(BF)
        x_moves[c] = over_x(
            lambda c, s: xsend.at[c, s], lambda c, s: rows.at[c, 0, s], c, xl_sem, x_ss, x_rs
        )

    def stage_x(c):
        arrived(x_moves[c])
        near[c] = (
            send(rows.at[c, 0], rows.at[c, 1], y_ss.at[c, 0], y_rs.at[c, 0], right),
            send(rows.at[c, 0], rows.at[c, 3], y_ss.at[c, 1], y_rs.at[c, 1], left),
        )

    def stage_near(c):
        near[c][0].wait_recv()
        one = send(rows.at[c, 1, high], rows.at[c, 2, high], y_ss.at[c, 2], y_rs.at[c, 2], right)
        near[c][1].wait_recv()
        two = send(rows.at[c, 3, low], rows.at[c, 2, low], y_ss.at[c, 3], y_rs.at[c, 3], left)
        far[c] = (one, two)

    def stage_gate(c):
        for copy in far[c]:
            copy.wait_recv()
        if c == 0:
            loads[2].wait()
            loads[3].wait()

        def tile(n, carry):
            to = pl.ds(pl.multiple_of(n * 256, 256), 256)
            part = mm(rows[c].reshape(NT * ROWS, LANES), w_in[lanes(c), to])
            if c % PARTS == 0:
                accum[:, to] = part
            else:
                accum[:, to] += part
            return carry

        lax.fori_loop(0, 2 * HID // 256, tile, 0)

    def stage_act(s):
        def some(b, carry):
            part = pl.ds(pl.multiple_of(b * 64, 64), 64)
            hidden[part] = (jax.nn.silu(accum[part, :HID]) * accum[part, HID:]).astype(BF)
            return carry

        lax.fori_loop(0, NT * ROWS // 64, some, 0)
        if s == 0:
            loads[4].wait()

    def stage_down(c):
        def tile(n, carry):
            to = pl.ds(pl.multiple_of(n * 256, 256), 256)
            at_lane = pl.ds(pl.multiple_of(c % PARTS * LANES + n * 256, 256), 256)
            part = mm(hidden[...], w_out[:, at_lane]).astype(BF)
            pbuf[c, :, :, to] = part.reshape(NT, ROWS, 256)
            return carry

        lax.fori_loop(0, LANES // 256, tile, 0)
        sums[c] = [
            send(pbuf.at[c, 2, high], relay.at[c, 0], r_ss.at[c, 0], r_rs.at[c, 0], right),
            send(pbuf.at[c, 2, low], relay.at[c, 1], r_ss.at[c, 1], r_rs.at[c, 1], left),
            send(pbuf.at[c, 3, low], ring.at[c, 0, low], r_ss.at[c, 2], r_rs.at[c, 2], right),
            send(pbuf.at[c, 1, high], ring.at[c, 1, high], r_ss.at[c, 3], r_rs.at[c, 3], left),
        ]

    def stage_join(c):
        sums[c][0].wait_recv()
        pbuf[c, 3, :HALF] = (
            pbuf[c, 3, :HALF].astype(F32) + relay[c, 0].astype(F32)
        ).astype(BF)
        one = send(pbuf.at[c, 3, high], ring.at[c, 0, high], r_ss.at[c, 4], r_rs.at[c, 4], right)
        sums[c][1].wait_recv()
        pbuf[c, 1, HALF:] = (
            pbuf[c, 1, HALF:].astype(F32) + relay[c, 1].astype(F32)
        ).astype(BF)
        two = send(pbuf.at[c, 1, low], ring.at[c, 1, low], r_ss.at[c, 5], r_rs.at[c, 5], left)
        joined[c] = (one, two)

    def stage_sum(c):
        for copy in sums[c][2:] + list(joined[c]):
            copy.wait_recv()
        ebuf[c] = (
            pbuf[c, 0].astype(F32) + ring[c, 0].astype(F32) + ring[c, 1].astype(F32)
        ).astype(BF)
        back_x[c] = over_x(
            lambda c, s: ebuf.at[c, s], lambda c, s: xback.at[c, s], c, bl_sem, bx_ss, bx_rs
        )

    def stage_back(c):
        arrived(back_x[c])
        zsend[c] = mm(order_back, xback[c]).astype(BF)
        back_z[c] = over_z(zsend, zback, c, cl_sem, bz_ss, bz_rs)

    def stage_pick(c):
        arrived(back_z[c])
        s = c // PARTS
        part = share[0] * mm(picking(0, s), zback[c]) + share[1] * mm(picking(1, s), zback[c])
        if s == 0:
            branch_ref[:, lanes(c)] = part
        else:
            branch_ref[:, lanes(c)] += part

    stages = {
        "z": stage_z,
        "x": stage_x,
        "near": stage_near,
        "gate": stage_gate,
        "act": stage_act,
        "down": stage_down,
        "join": stage_join,
        "sum": stage_sum,
        "back": stage_back,
        "pick": stage_pick,
    }
    for name, c in events():
        stages[name](c)

    for moves in (z_moves, x_moves, back_x, back_z):
        for copies, _ in moves.values():
            for copy in copies.values():
                copy.wait_send()
    for group in (near, far, sums, joined):
        for copies in group.values():
            for copy in copies:
                copy.wait_send()
    for group in (fwd, bwd, across, qcopies, ocopies, hcopies):
        for copy in group.values():
            copy.wait_send()
    for copy in wcopies:
        copy.wait_send()


def layer(*args):
    dma = pltpu.SemaphoreType.DMA
    vmem = pl.BlockSpec(memory_space=pltpu.VMEM)
    hbm = pl.BlockSpec(memory_space=pl.ANY)
    buf = pltpu.VMEM((CHUNKS, ROWS, LANES), BF)
    return pl.pallas_call(
        layer_kernel,
        out_shape=(
            jax.ShapeDtypeStruct((SUB, D), F32),
            jax.ShapeDtypeStruct((SUB, D), BF),
        ),
        in_specs=[vmem] * 16 + [hbm] * 5,
        out_specs=(vmem, vmem),
        scratch_shapes=[
            pltpu.VMEM((NX, TOK, 384), BF),
            pltpu.VMEM((NZ, NC, TOK + ROPE, 256), BF),
            pltpu.VMEM((256, 512), BF),
            pltpu.VMEM((6 * TOK, 256), BF),
            pltpu.VMEM((6 * TOK, 128), BF),
            pltpu.VMEM((6 * TOK, 256), BF),
            pltpu.VMEM((6 * TOK, 128), BF),
            pltpu.VMEM((NX, TOK, 128), F32),
            pltpu.VMEM((NX, TOK, 128), F32),
            pltpu.VMEM((NX, TOK, 256), F32),
            pltpu.VMEM((NX, TOK, 128), F32),
            pltpu.VMEM((NX, TOK, 256), BF),
            pltpu.VMEM((NX, TOK, 256), BF),
            pltpu.VMEM((TOK, 256), BF),
            pltpu.VMEM((NT, SUB, 256), BF),
            pltpu.VMEM((NT, 192, D), BF),
            pltpu.VMEM((SUB, D), BF),
            buf,
            buf,
            buf,
            pltpu.VMEM((CHUNKS, NT, ROWS, LANES), BF),
            pltpu.VMEM((D, 2 * HID), BF),
            pltpu.VMEM((HID, D), BF),
            pltpu.VMEM((NT * ROWS, 2 * HID), F32),
            pltpu.VMEM((NT * ROWS, HID), BF),
            pltpu.VMEM((CHUNKS, NT, ROWS, LANES), BF),
            pltpu.VMEM((CHUNKS, 2, HALF, LANES), BF),
            pltpu.VMEM((CHUNKS, 2, ROWS, LANES), BF),
            buf,
            buf,
            buf,
            buf,
            dma((5,)),
            dma((NX,)),
            dma((NX,)),
            dma((5,)),
            dma((5,)),
            dma((5,)),
            dma((5,)),
            dma((9,)),
            dma((9,)),
            dma((NX,)),
            dma((NX,)),
            dma((NT,)),
            dma((NT,)),
            dma((4,)),
            dma((4,)),
            dma((CHUNKS,)),
            dma((CHUNKS, NZ)),
            dma((CHUNKS, NZ)),
            dma((CHUNKS,)),
            dma((CHUNKS, GROUP)),
            dma((CHUNKS, GROUP)),
            dma((CHUNKS, 4)),
            dma((CHUNKS, 4)),
            dma((CHUNKS, 6)),
            dma((CHUNKS, 6)),
            dma((CHUNKS,)),
            dma((CHUNKS, GROUP)),
            dma((CHUNKS, GROUP)),
            dma((CHUNKS,)),
            dma((CHUNKS, NZ)),
            dma((CHUNKS, NZ)),
        ],
        compiler_params=pltpu.CompilerParams(
            collective_id=0, has_side_effects=True, vmem_limit_bytes=58 * 1024 * 1024
        ),
        name="layer",
    )(*args)


def local(
    resid,
    query_wide,
    query_narrow,
    latent,
    rope_key,
    latent_gain,
    key_up_wide,
    value_up_wide,
    key_up_narrow,
    value_up_narrow,
    out_wide,
    out_narrow,
    attn_gain,
    ffn_gain,
    moe_gain,
    routes,
    route_logit,
    expert_gate,
    expert_up,
    expert_down,
):
    positions = lax.axis_index(SP) * TOK + jnp.arange(TOK, dtype=jnp.int32)
    freq = THETA ** (-jnp.arange(ROPE // 2, dtype=jnp.float32) * 2.0 / ROPE)
    angle = freq[:, None] * positions.astype(jnp.float32)[None, :]
    branch, stream = layer(
        latent,
        latent_gain[None],
        rope_key.T,
        query_wide.T,
        query_narrow.T,
        jnp.cos(angle),
        jnp.sin(angle),
        key_up_wide,
        value_up_wide,
        key_up_narrow,
        value_up_narrow,
        resid,
        attn_gain[None],
        ffn_gain[None],
        routes.T,
        route_logit.T,
        out_wide,
        out_narrow,
        expert_gate,
        expert_up,
        expert_down,
    )
    return (stream.astype(jnp.float32) + rms_scale(branch, moe_gain)).astype(jnp.bfloat16)


def solution(mesh):
    split = Mesh(mesh.devices.reshape(8, 4, 2, mesh.shape["tp"]), ("sp_0", "sp_1", "sp_2", "tp"))
    in_specs = (
        P(SP_TP, None),
        P(SP, "tp"),
        P(SP, "tp"),
        P(SP, None),
        P(SP, None),
        P(),
        P(),
        P(),
        P(),
        P(),
        P("tp", None),
        P("tp", None),
        P(),
        P(),
        P(),
        P(SP_TP, None),
        P(SP_TP, None),
        P(SP, None, "tp"),
        P(SP, None, "tp"),
        P(SP, "tp", None),
    )
    out_specs = P(SP_TP, None)
    return jax.shard_map(local, mesh=split, in_specs=in_specs, out_specs=out_specs, check_vma=False)
```

time: 423 us -> 154 us (0.36); the launches traced: 418 us -> 154 us
  Pallas kernels: 0 us -> 148 us
  waiting for transfers between devices: 124 us -> 0 us
  blocking collectives: 122 us -> 0 us
  matrix products: 93.3 us -> 0 us
  local copies, waits for them, and re-layouts: 26.3 us -> 1.58 us
  other arithmetic: 27.9 us -> 4 us
  between operations: 14 us -> 0.03 us
  starting transfers between devices: 10.7 us -> 0 us
    pallas_call x0 -> x1, Pallas kernels: none -> 148 us  [layer(): pl.pallas_call(layer_kernel, out_shape=(jax.ShapeDtypeStruct((SUB, D), F3...]
    all_to_all x4 -> x0, blocking collectives: 122 us -> none  [the longest x1 39.2 us: sent_to_all(): return lax.all_to_all(copies, axis, split_axis=0, concat_axis=0, tiled=True)]
    dot_general x12 -> x0, matrix products: 93.3 us -> none  [the longest x4 50.7 us: contract(): lax.dot_general(left, right, (((1,), (1,)), ((), ())), preferred_element_...]
    all_gather x1 -> x0, waiting for transfers between devices: 91.2 us -> none  [sent_together(): result = lax.all_gather(both, axis, axis=dim, tiled=True)]
    all_to_all x2 -> x0, waiting for transfers between devices: 32.9 us -> none  [the longest x1 19.2 us: moved_by_axis(): result = lax.all_to_all(result, axes[k], k, k, tiled=True)]
    reduce_sum x7 -> x0, other arithmetic: 20.6 us -> none  [the longest x2 16.2 us: attend(): weight_sum = weight_sum * shrink + jnp.sum(weights, axis=1)]
    another operation x6 -> x0, local copies, waits for them, and re-layouts: 11.7 us -> none  [the longest x1 8.81 us: local(): flat = gathered.reshape(-1, gathered.shape[2])]
    all_to_all x2 -> x0, starting transfers between devices: 10.7 us -> none  [the longest x1 6.73 us: moved_by_axis(): result = lax.all_to_all(result, axes[k], k, k, tiled=True)]
  transfers between devices with their start and end apart: 3 -> 0, of which waited for: 3 -> 0; matrix products, arithmetic and copies ran while one was open for 1% -> 0% of each run, Pallas kernels for 0% -> 0%
where the time goes in v2:
time: 154 us
  Pallas kernels  148 us (96%)
  other arithmetic  4 us (3%)
  local copies, waits for them, and re-layouts  1.58 us (1%)
    pallas_call x1, Pallas kernels, layer(): pl.pallas_call(layer_kernel, out_shape=(jax.ShapeDtypeStruct((SUB, D), F3...  148 us

profile of v2, /device:TPU:1, one launch (start us, length us, event | category | flops | bytes accessed | tf_op | source)
XLA Modules:
  0.0 154.0 jit_solution(8157810881091911677)
XLA Ops:
  0.0 0.8 multiply_sine_fusion
  0.9 1.6 %copy.21 = bf16[256,128]{0,1:T(8,128)(2,1)} copy(bf16[256,128]{1,0:T(8,128)(2,1)} %param.22) | data formatting | bytes 131072 | tf_op args[2]
  2.4 0.0 copy-start
  2.4 148.4 %layer.1 = (f32[64,2048]{1,0:T(8,128)}, bf16[64,2048]{1,0:T(8,128)(2,1)}) custom-call(bf16[256,256]{1,0:T(8,128)(2,1)} %latent.1, f32[1,256]{1,0:T(1,128)} %bitcast.13, bf16[64,256]{1,0:T(8,128)(2,1)} %bitcast.10, bf16[192,256]{1,0:T(8,128)(2,1)} %bitcast.9, bf16[128,256]{1,0:T(8,128)(2,1)} %bitcast.8, f32[32,256]{1,0:T(8,128)} %get-tuple-element.10.cosine, ...), custom_call_target="tpu_custom_call" | custom-call | tf_op jit(solution)/shard_map/layer/pallas_call | solution.py:696
  150.8 1.2 multiply_reduce_fusion
  152.0 0.0 copy-done
  152.0 2.0 %add_convert_fusion = bf16[64,2048]{1,0:T(8,128)(2,1)} fusion(f32[64,2048]{1,0:T(8,128)} %get-tuple-element.8, bf16[64,2048]{1,0:T(8,128)(2,1)} %get-tuple-element.7, f32[2048]{0:T(1024)S(1)} %copy-done, f32[64]{0:T(128)S(1)} %add_rsqrt_fusion), kind=kLoop, calls=%fused_computation | loop fusion | flops 655360 | bytes 1057024 | tf_op jit(solution)/shard_map/convert_element_type | solution.py:824
  (3 shorter events, 0.0 us)
Async XLA Ops:
  2.4 149.6 %copy-start = (f32[2048]{0:T(1024)S(1)}, f32[2048]{0:T(1024)}, u32[]{:S(2)}) copy-start(f32[2048]{0:T(1024)} %param.34) | copy-start | bytes 24580

commit v3 on v2

--- a/solution.py
+++ b/solution.py
@@ -71,33 +71,23 @@
     return values * lax.rsqrt(jnp.mean(values * values, axis=-1, keepdims=True) + EPS) * gain
 
 
-def events():
-    out = []
-    z_step, y_step = 7.0 / PARTS, 8.4 / PARTS
-    for c in range(CHUNKS):
-        at_z = 3 + z_step * (c + 1)
-        at_x = at_z + 4
-        near = max(at_x + 5, 10.5 + 4 + y_step * c)
-        out.append((at_z, 0, "z", c))
-        out.append((at_x, 1, "x", c))
-        out.append((near, 2, "near", c))
-        out.append((near + 3.5, 3, "gate", c))
-    last = 0.0
-    for s in range(SLOTS):
-        ready = max(at for at, _, name, c in out if name == "gate" and c == s * PARTS + PARTS - 1)
-        out.append((ready + 0.1, 4, "act", s))
-        for h in range(PARTS):
-            c = s * PARTS + h
-            down = ready + 0.2 + 0.01 * h
-            join = max(down + 5, last + y_step)
-            done = join + 4
-            last = join
-            out.append((down, 5, "down", c))
-            out.append((join, 6, "join", c))
-            out.append((done, 7, "sum", c))
-            out.append((done + 4, 8, "back", c))
-            out.append((done + 10, 9, "pick", c))
-    return [(name, c) for _, _, name, c in sorted(out)]
+STAGES = (
+    "z0 z1 x0 z2",
+    "x1 z3 near0 x2",
+    "z4 near1 x3 gate0",
+    "z5 x4 near2 gate1",
+    "act0 down0 near3 x5",
+    "down1 near4 gate2 join0",
+    "near5 gate3 act1 down2",
+    "join1 down3 gate4 sum0",
+    "join2 gate5 join3 back0",
+    "act2 down4 down5 sum1",
+    "sum2 sum3 pick0 join4",
+    "back1 back2 join5 back3",
+    "sum4 pick1 sum5 pick2",
+    "back4 back5 pick3 pick4",
+    "pick5",
+)
 
 
 def layer_kernel(
@@ -105,7 +95,7 @@
     latent_gain,
     rope_t,
     wide_t,
-    narrow_t,
+    narrow_q,
     cosine,
     sine,
     key_wide,
@@ -115,6 +105,7 @@
     resid,
     attn_gain,
     ffn_gain,
+    moe_gain,
     routes_t,
     logit_t,
     out_wide,
@@ -122,8 +113,8 @@
     gate_hbm,
     up_hbm,
     down_hbm,
+    mixed_ref,
     branch_ref,
-    stream_ref,
     qbuf,
     kvbuf,
     w_kv,
@@ -229,12 +220,13 @@
 
     kvbuf[0, 0, :TOK] = rms_scale(latent[...].astype(F32), latent_gain[...]).astype(BF)
     kvbuf[0, 0, TOK:] = turn(rope_t[...]).astype(BF)
+    narrow_t = narrow_q[...].astype(F32).T
     qbuf[0, :, :128] = wide_t[:128].astype(F32).T.astype(BF)
     qbuf[0, :, 128:256] = (
         jnp.concatenate([turn(wide_t[128:]), jnp.zeros((64, TOK), F32)], axis=0).T.astype(BF)
     )
     qbuf[0, :, 256:] = (
-        jnp.concatenate([narrow_t[:64].astype(F32), turn(narrow_t[64:])], axis=0).T.astype(BF)
+        jnp.concatenate([narrow_t[:64], turn(narrow_t[64:])], axis=0).T.astype(BF)
     )
 
     pl.semaphore_wait(barrier, len(peers))
@@ -334,7 +326,7 @@
 
     lane_q = lax.broadcasted_iota(jnp.int32, (TOK, 128), 1)
 
-    def expand(base, count):
+    def expand(base, begin, end):
         def one(i, carry):
             piece = kvbuf[base + i // NC, lax.rem(i, NC)]
             to = pl.ds(pl.multiple_of(i * TOK, TOK), TOK)
@@ -348,7 +340,7 @@
             vn_s[to] = jnp.where(lane_q < 64, full[:, 384:], 1.0).astype(BF)
             return carry
 
-        lax.fori_loop(0, count * NC, one, 0)
+        lax.fori_loop(begin, end, one, 0)
 
     def one_head(q, keys, values, top, acc, j, factor, fresh):
         scores = mm_nt(q, keys)
@@ -382,10 +374,15 @@
         bwd[k + 1].start()
         across[NZ - k].start()
 
+    expand(0, 0, 1)
+    across[0].wait_recv()
+    expand(0, 1, 2)
     forward(1)
-    for r in (0, 1, 7):
-        across[r].wait_recv()
-    expand(0, 3)
+    expand(0, 2, 3)
+    across[1].wait_recv()
+    expand(0, 3, 5)
+    across[7].wait_recv()
+    expand(0, 5, 6)
 
     def first_body(j, carry):
         for other in range(1, NX):
@@ -405,7 +402,7 @@
     lax.fori_loop(0, NX, first_body, 0)
     for r in (2, 6):
         across[r].wait_recv()
-    expand(3, 2)
+    expand(3, 0, 4)
 
     def second_body(j, carry):
         attend(j, 2, False)
@@ -427,7 +424,7 @@
     across[8].start()
     for r in (3, 5, 4, 8):
         across[r].wait_recv()
-    expand(5, 3)
+    expand(5, 0, 6)
 
     def three(value):
         high = value.astype(BF).astype(F32)
@@ -453,7 +450,7 @@
     }
 
     def last_body(i, carry):
-        j = NX - 1 - i
+        j = 2 + i - i // 2 * (2 * i - 1)
         attend(j, 3, False)
         finish(j)
         for other in range(1, NX):
@@ -465,7 +462,7 @@
         return carry
 
     lax.fori_loop(0, NX, last_body, 0)
-    for j in (3, 2, 1):
+    for j in (2, 3, 1):
         ocopies[j].wait_recv()
 
     tails = [osend[0, :, 128:].astype(F32)] + [orecv[j, :, 128:].astype(F32) for j in (1, 2, 3)]
@@ -496,7 +493,7 @@
         hcopies[j].wait_recv()
         proj = proj + mm(yrecv[j, :, :192], wbuf[j]).astype(BF).astype(F32)
     stream = (resid[...].astype(F32) + rms_scale(proj, attn_gain[...])).astype(BF)
-    stream_ref[...] = stream
+    mixed_ref[...] = stream
     moe_in[...] = rms_scale(stream.astype(F32), ffn_gain[...]).astype(BF)
 
     z_order = (4, 3, 5, 2, 6, 1, 7)
@@ -585,7 +582,7 @@
             loads[3].wait()
 
         def tile(n, carry):
-            to = pl.ds(pl.multiple_of(n * 256, 256), 256)
+            to = pl.ds(pl.multiple_of(n * HID, 128), HID)
             part = mm(rows[c].reshape(NT * ROWS, LANES), w_in[lanes(c), to])
             if c % PARTS == 0:
                 accum[:, to] = part
@@ -593,7 +590,7 @@
                 accum[:, to] += part
             return carry
 
-        lax.fori_loop(0, 2 * HID // 256, tile, 0)
+        lax.fori_loop(0, 2, tile, 0)
 
     def stage_act(s):
         def some(b, carry):
@@ -670,8 +667,13 @@
         "back": stage_back,
         "pick": stage_pick,
     }
-    for name, c in events():
-        stages[name](c)
+    for line in STAGES:
+        for word in line.split():
+            stages[word[:-1]](int(word[-1]))
+
+    mixed_ref[...] = (
+        mixed_ref[...].astype(F32) + rms_scale(branch_ref[...], moe_gain[...])
+    ).astype(BF)
 
     for moves in (z_moves, x_moves, back_x, back_z):
         for copies, _ in moves.values():
@@ -695,13 +697,11 @@
     buf = pltpu.VMEM((CHUNKS, ROWS, LANES), BF)
     return pl.pallas_call(
         layer_kernel,
-        out_shape=(
-            jax.ShapeDtypeStruct((SUB, D), F32),
-            jax.ShapeDtypeStruct((SUB, D), BF),
-        ),
-        in_specs=[vmem] * 16 + [hbm] * 5,
-        out_specs=(vmem, vmem),
+        out_shape=jax.ShapeDtypeStruct((SUB, D), BF),
+        in_specs=[vmem] * 17 + [hbm] * 5,
+        out_specs=vmem,
         scratch_shapes=[
+            pltpu.VMEM((SUB, D), F32),
             pltpu.VMEM((NX, TOK, 384), BF),
             pltpu.VMEM((NZ, NC, TOK + ROPE, 256), BF),
             pltpu.VMEM((256, 512), BF),
@@ -798,12 +798,12 @@
     positions = lax.axis_index(SP) * TOK + jnp.arange(TOK, dtype=jnp.int32)
     freq = THETA ** (-jnp.arange(ROPE // 2, dtype=jnp.float32) * 2.0 / ROPE)
     angle = freq[:, None] * positions.astype(jnp.float32)[None, :]
-    branch, stream = layer(
+    return layer(
         latent,
         latent_gain[None],
         rope_key.T,
         query_wide.T,
-        query_narrow.T,
+        query_narrow,
         jnp.cos(angle),
         jnp.sin(angle),
         key_up_wide,
@@ -813,6 +813,7 @@
         resid,
         attn_gain[None],
         ffn_gain[None],
+        moe_gain[None],
         routes.T,
         route_logit.T,
         out_wide,
@@ -821,7 +822,6 @@
         expert_up,
         expert_down,
     )
-    return (stream.astype(jnp.float32) + rms_scale(branch, moe_gain)).astype(jnp.bfloat16)
 
 
 def solution(mesh):

time: 154 us -> 136 us (0.88)
  Pallas kernels: 148 us -> 133 us
  other arithmetic: 4 us -> 0.84 us
    pallas_call x1, Pallas kernels: 148 us -> 133 us  [layer(): pl.pallas_call(layer_kernel, out_shape=jax.ShapeDtypeStruct((SUB, D), BF)...]
    convert_element_type x1 -> x0, other arithmetic: 1.96 us -> none  [local(): (stream.astype(jnp.float32) + rms_scale(branch, moe_gain)).astype(jnp.bfl...]
where the time goes in v3:
time: 136 us
  Pallas kernels  133 us (98%)
  local copies, waits for them, and re-layouts  1.67 us (1%)
    pallas_call x1, Pallas kernels, layer(): pl.pallas_call(layer_kernel, out_shape=jax.ShapeDtypeStruct((SUB, D), BF)...  133 us

profile of v3, /device:TPU:1, one launch (start us, length us, event | category | flops | bytes accessed | tf_op | source)
XLA Modules:
  0.0 135.5 jit_solution(13971878429097343196)
XLA Ops:
  0.0 0.8 multiply_sine_fusion
  0.8 133.0 %layer.1 = bf16[64,2048]{1,0:T(8,128)(2,1)} custom-call(bf16[256,256]{1,0:T(8,128)(2,1)} %latent.1, f32[1,256]{1,0:T(1,128)} %bitcast.13, bf16[64,256]{1,0:T(8,128)(2,1)} %bitcast.9, bf16[192,256]{1,0:T(8,128)(2,1)} %bitcast.8, bf16[256,128]{1,0:T(8,128)(2,1)} %narrow_q.1, f32[32,256]{1,0:T(8,128)} %get-tuple-element.6.cosine, ...), custom_call_target="tpu_custom_call" | custom-call | tf_op jit(solution)/shard_map/layer/pallas_call | solution.py:698
  133.9 1.7 %copy.22 = bf16[64,2048]{1,0:T(8,128)(2,1)} copy(bf16[64,2048]{1,0:T(8,128)(2,1)} %layer.1) | data formatting | bytes 524288
  (2 shorter events, 0.0 us)

commit v4 on v3

--- a/solution.py
+++ b/solution.py
@@ -26,9 +26,13 @@
 
 GROUP = NX * NC
 SLOTS = 3
-PARTS = 2
-LANES = D // PARTS
-CHUNKS = SLOTS * PARTS
+WIDE = 1024
+PIECES = tuple(
+    [(0, n * 512, 512) for n in range(4)]
+    + [(1, n * 1024, 1024) for n in range(2)]
+    + [(2, n * 512, 512) for n in range(4)]
+)
+CHUNKS = len(PIECES)
 ROWS = NZ * GROUP
 HID = 896
 HALF = ROWS // 2
@@ -72,21 +76,30 @@
 
 
 STAGES = (
-    "z0 z1 x0 z2",
-    "x1 z3 near0 x2",
-    "z4 near1 x3 gate0",
-    "z5 x4 near2 gate1",
-    "act0 down0 near3 x5",
-    "down1 near4 gate2 join0",
-    "near5 gate3 act1 down2",
-    "join1 down3 gate4 sum0",
-    "join2 gate5 join3 back0",
-    "act2 down4 down5 sum1",
-    "sum2 sum3 pick0 join4",
-    "back1 back2 join5 back3",
-    "sum4 pick1 sum5 pick2",
-    "back4 back5 pick3 pick4",
-    "pick5",
+    "z0 z1 z2 x0",
+    "z3 x1 x2 z4",
+    "x3 near0 near1 near2",
+    "z5 near3 x4 z8",
+    "x5 gate2 gate3 z9",
+    "x8 gate0 near4 gate1",
+    "z6 z7 act0 near5",
+    "down2 down3 x7 down1",
+    "x9 near8 gate4 down0",
+    "gate5 join3 near9 x6",
+    "act1 down4 gate9 join1",
+    "gate8 near6 sum3 join4",
+    "near7 down5 join2 join0",
+    "gate6 sum4 sum1 gate7",
+    "join5 act2 down7 back3",
+    "sum2 back4 down6 sum0",
+    "down9 sum5 back1 back2",
+    "join7 back0 join6 down8",
+    "back5 join9 sum7 sum6",
+    "join8 sum9 pick0 pick3",
+    "back7 sum8 pick1 back6",
+    "back9 pick4 back8 pick7",
+    "pick6 pick2 pick5 pick9",
+    "pick8",
 )
 
 
@@ -115,6 +128,8 @@
     down_hbm,
     mixed_ref,
     branch_ref,
+    nbuf,
+    rbuf,
     qbuf,
     kvbuf,
     w_kv,
@@ -210,7 +225,16 @@
         pltpu.make_async_copy(up_hbm.at[0], w_in.at[:, pl.ds(HID, HID)], l_sem.at[3]),
         pltpu.make_async_copy(down_hbm.at[0], w_out, l_sem.at[4]),
     ]
-    for load in loads:
+    wide_at = pl.ds(pl.multiple_of(y * 128, 128), 128)
+    narrow_at = pl.ds(pl.multiple_of(y // 2 * 128, 128), 128)
+    ahead = [
+        pltpu.make_async_copy(key_wide.at[:, wide_at], w_kv.at[:, pl.ds(0, 128)], l_sem.at[5]),
+        pltpu.make_async_copy(value_wide.at[:, wide_at], w_kv.at[:, pl.ds(256, 128)], l_sem.at[6]),
+        pltpu.make_async_copy(key_narrow.at[:, narrow_at], nbuf.at[0], l_sem.at[7]),
+        pltpu.make_async_copy(value_narrow.at[:, narrow_at], nbuf.at[1], l_sem.at[8]),
+        pltpu.make_async_copy(resid, rbuf, l_sem.at[9]),
+    ]
+    for load in ahead + loads:
         load.start()
 
     def turn(values):
@@ -231,26 +255,31 @@
 
     pl.semaphore_wait(barrier, len(peers))
 
-    half = 160
+    halves = (pl.ds(0, 160), pl.ds(160, 160))
+    first, second = halves
     fwd, bwd, across = {}, {}, {}
 
     def at(r):
         return SLOT_OF[r % NZ]
 
-    for k in range(1, 4):
-        fwd[k] = plan(
-            kvbuf.at[at(k - 1), 0], kvbuf.at[at(k), 0], f_ss.at[k], f_rs.at[k], up
-        )
-        bwd[k] = plan(
-            kvbuf.at[at(1 - k), 0], kvbuf.at[at(-k), 0], b_ss.at[k], b_rs.at[k], down
-        )
-    first, second = pl.ds(0, half), pl.ds(half, half)
-    fwd[4] = plan(
-        kvbuf.at[at(3), 0, first], kvbuf.at[at(4), 0, first], f_ss.at[4], f_rs.at[4], up
-    )
-    bwd[4] = plan(
-        kvbuf.at[at(5), 0, second], kvbuf.at[at(4), 0, second], b_ss.at[4], b_rs.at[4], down
-    )
+    for k in range(1, 5):
+        for h, part in enumerate(halves):
+            if k < 4 or h == 0:
+                fwd[k, h] = plan(
+                    kvbuf.at[at(k - 1), 0, part],
+                    kvbuf.at[at(k), 0, part],
+                    f_ss.at[k, h],
+                    f_rs.at[k, h],
+                    up,
+                )
+            if k < 4 or h == 1:
+                bwd[k, h] = plan(
+                    kvbuf.at[at(1 - k), 0, part],
+                    kvbuf.at[at(-k), 0, part],
+                    b_ss.at[k, h],
+                    b_rs.at[k, h],
+                    down,
+                )
     for r in (0, 1, 2, 3, 5, 6, 7):
         across[r] = plan(
             kvbuf.at[at(r), 0], kvbuf.at[at(r), 1], d_ss.at[r], d_rs.at[r], sibling
@@ -261,8 +290,9 @@
     across[8] = plan(
         kvbuf.at[at(4), 0, second], kvbuf.at[at(4), 1, second], d_ss.at[8], d_rs.at[8], sibling
     )
-    fwd[1].start()
-    bwd[1].start()
+    for h in range(2):
+        fwd[1, h].start()
+        bwd[1, h].start()
     across[0].start()
     qcopies = {
         j: send(qbuf.at[0], qbuf.at[j], q_ss.at[j], q_rs.at[j], xs[j]) for j in (1, 3, 2)
@@ -280,18 +310,15 @@
     wcopies[1].start()
 
     lane_w = lax.broadcasted_iota(jnp.int32, (256, 128), 1)
-    wide_at = pl.ds(pl.multiple_of(y * 128, 128), 128)
-    narrow_at = pl.ds(pl.multiple_of(y // 2 * 128, 128), 128)
     odd = lax.rem(y, 2) == 1
 
-    def narrow(ref):
-        both = ref[:, narrow_at].astype(F32)
+    def narrow(both):
         return jnp.where(lane_w < 64, jnp.where(odd, pltpu.roll(both, 64, 1), both), 0.0)
 
-    w_kv[:, :128] = key_wide[:, wide_at]
-    w_kv[:, 128:256] = narrow(key_narrow).astype(BF)
-    w_kv[:, 256:384] = value_wide[:, wide_at]
-    w_kv[:, 384:] = narrow(value_narrow).astype(BF)
+    for load in ahead:
+        load.wait()
+    w_kv[:, 128:256] = narrow(nbuf[0].astype(F32)).astype(BF)
+    w_kv[:, 384:] = narrow(nbuf[1].astype(F32)).astype(BF)
     vw_s[:, 128:] = jnp.ones((6 * TOK, 128), BF)
 
     expert = lax.broadcasted_iota(jnp.int32, (SUB, SUB), 0)
@@ -367,11 +394,12 @@
         one_head(q[:, 256:], kn_s[:keys], vn_s[:keys], top_n, acc_n, j, FACTOR_N, fresh)
 
     def forward(k):
-        fwd[k].wait_recv()
-        fwd[k + 1].start()
+        for h in range(2):
+            for ring_way in (fwd, bwd):
+                ring_way[k, h].wait_recv()
+                if (k + 1, h) in ring_way:
+                    ring_way[k + 1, h].start()
         across[k].start()
-        bwd[k].wait_recv()
-        bwd[k + 1].start()
         across[NZ - k].start()
 
     expand(0, 0, 1)
@@ -407,9 +435,12 @@
     def second_body(j, carry):
         attend(j, 2, False)
 
+        @pl.when(j == 0)
+        def _():
+            forward(3)
+
         @pl.when(j == 1)
         def _():
-            forward(3)
             wcopies[0].wait_recv()
             wcopies[2].start()
             wcopies[1].wait_recv()
@@ -418,13 +449,16 @@
         return carry
 
     lax.fori_loop(0, NX, second_body, 0)
-    fwd[4].wait_recv()
+    for r in (3, 5):
+        across[r].wait_recv()
+    expand(5, 0, 4)
+    fwd[4, 0].wait_recv()
     across[4].start()
-    bwd[4].wait_recv()
+    bwd[4, 1].wait_recv()
     across[8].start()
-    for r in (3, 5, 4, 8):
+    for r in (4, 8):
         across[r].wait_recv()
-    expand(5, 0, 6)
+    expand(5, 4, 6)
 
     def three(value):
         high = value.astype(BF).astype(F32)
@@ -492,7 +526,7 @@
                 wcopies[copy].wait_recv()
         hcopies[j].wait_recv()
         proj = proj + mm(yrecv[j, :, :192], wbuf[j]).astype(BF).astype(F32)
-    stream = (resid[...].astype(F32) + rms_scale(proj, attn_gain[...])).astype(BF)
+    stream = (rbuf[...].astype(F32) + rms_scale(proj, attn_gain[...])).astype(BF)
     mixed_ref[...] = stream
     moe_in[...] = rms_scale(stream.astype(F32), ffn_gain[...]).astype(BF)
 
@@ -501,19 +535,24 @@
 
     def seg(number):
         return pl.ds(pl.multiple_of(number * 8, 8), 8)
+
+    def across_lanes(c):
+        return pl.ds(0, PIECES[c][2])
 
     def over_z(src, dst, c, local_sem, ss, rs):
         copies = {
             d: send(
-                src.at[c, seg(zs[d])],
-                dst.at[c, seg(z)],
+                src.at[c, seg(zs[d]), across_lanes(c)],
+                dst.at[c, seg(z), across_lanes(c)],
                 ss.at[c, d],
                 rs.at[c, d],
                 {"sp_0": zs[d]},
             )
             for d in z_order
         }
-        kept = pltpu.make_async_copy(src.at[c, seg(z)], dst.at[c, seg(z)], local_sem.at[c])
+        kept = pltpu.make_async_copy(
+            src.at[c, seg(z), across_lanes(c)], dst.at[c, seg(z), across_lanes(c)], local_sem.at[c]
+        )
         kept.start()
         return copies, kept
 
@@ -539,52 +578,73 @@
             copy.wait_recv()
 
     def lanes(c):
-        h = c % PARTS
-        return slice(h * LANES, (h + 1) * LANES)
+        return slice(PIECES[c][1], PIECES[c][1] + PIECES[c][2])
+
+    def here(c):
+        return slice(0, PIECES[c][2])
 
     z_moves, x_moves, near, far = {}, {}, {}, {}
     sums, joined, back_x, back_z = {}, {}, {}, {}
-    high, low = pl.ds(0, HALF), pl.ds(HALF, HALF)
-
-    for s in range(SLOTS):
-        place = placing(s).astype(BF)
-        for h in range(PARTS):
-            c = s * PARTS + h
-            sbuf[c] = mm(place, moe_in[:, lanes(c)]).astype(BF)
-            z_moves[c] = over_z(sbuf, zbuf, c, zl_sem, z_ss, z_rs)
+    high, low, whole = pl.ds(0, HALF), pl.ds(HALF, HALF), pl.ds(0, ROWS)
+    begun = set()
+
+    def hop(src, src_at, dst, dst_at, part, ss, rs, n, where):
+        c = src_at[0]
+        return send(
+            src.at[(*src_at, part, across_lanes(c))],
+            dst.at[(*dst_at, part, across_lanes(c))],
+            ss.at[c, n],
+            rs.at[c, n],
+            where,
+        )
+
+    branch_ref[...] = jnp.zeros((SUB, D), F32)
+    for c in range(CHUNKS):
+        place = placing(PIECES[c][0]).astype(BF)
+        sbuf[c, :, here(c)] = mm(place, moe_in[:, lanes(c)]).astype(BF)
+        z_moves[c] = over_z(sbuf, zbuf, c, zl_sem, z_ss, z_rs)
 
     def stage_z(c):
         arrived(z_moves[c])
-        xsend[c] = mm(order, zbuf[c]).astype(BF)
+        xsend[c, :, here(c)] = mm(order, zbuf[c, :, here(c)]).astype(BF)
         x_moves[c] = over_x(
-            lambda c, s: xsend.at[c, s], lambda c, s: rows.at[c, 0, s], c, xl_sem, x_ss, x_rs
+            lambda c, s: xsend.at[c, s, across_lanes(c)],
+            lambda c, s: rows.at[c, 0, s, across_lanes(c)],
+            c,
+            xl_sem,
+            x_ss,
+            x_rs,
         )
 
     def stage_x(c):
         arrived(x_moves[c])
         near[c] = (
-            send(rows.at[c, 0], rows.at[c, 1], y_ss.at[c, 0], y_rs.at[c, 0], right),
-            send(rows.at[c, 0], rows.at[c, 3], y_ss.at[c, 1], y_rs.at[c, 1], left),
+            hop(rows, (c, 0), rows, (c, 1), whole, y_ss, y_rs, 0, right),
+            hop(rows, (c, 0), rows, (c, 3), whole, y_ss, y_rs, 1, left),
         )
 
     def stage_near(c):
         near[c][0].wait_recv()
-        one = send(rows.at[c, 1, high], rows.at[c, 2, high], y_ss.at[c, 2], y_rs.at[c, 2], right)
+        one = hop(rows, (c, 1), rows, (c, 2), high, y_ss, y_rs, 2, right)
         near[c][1].wait_recv()
-        two = send(rows.at[c, 3, low], rows.at[c, 2, low], y_ss.at[c, 3], y_rs.at[c, 3], left)
+        two = hop(rows, (c, 3), rows, (c, 2), low, y_ss, y_rs, 3, left)
         far[c] = (one, two)
 
     def stage_gate(c):
         for copy in far[c]:
             copy.wait_recv()
-        if c == 0:
+        if not begun:
             loads[2].wait()
             loads[3].wait()
+        slot = PIECES[c][0]
+        fresh = slot not in begun
+        begun.add(slot)
 
         def tile(n, carry):
             to = pl.ds(pl.multiple_of(n * HID, 128), HID)
-            part = mm(rows[c].reshape(NT * ROWS, LANES), w_in[lanes(c), to])
-            if c % PARTS == 0:
+            held = rows[c, :, :, here(c)].reshape(NT * ROWS, PIECES[c][2])
+            part = mm(held, w_in[lanes(c), to])
+            if fresh:
                 accum[:, to] = part
             else:
                 accum[:, to] += part
@@ -605,55 +665,62 @@
     def stage_down(c):
         def tile(n, carry):
             to = pl.ds(pl.multiple_of(n * 256, 256), 256)
-            at_lane = pl.ds(pl.multiple_of(c % PARTS * LANES + n * 256, 256), 256)
+            at_lane = pl.ds(pl.multiple_of(PIECES[c][1] + n * 256, 256), 256)
             part = mm(hidden[...], w_out[:, at_lane]).astype(BF)
             pbuf[c, :, :, to] = part.reshape(NT, ROWS, 256)
             return carry
 
-        lax.fori_loop(0, LANES // 256, tile, 0)
+        lax.fori_loop(0, PIECES[c][2] // 256, tile, 0)
         sums[c] = [
-            send(pbuf.at[c, 2, high], relay.at[c, 0], r_ss.at[c, 0], r_rs.at[c, 0], right),
-            send(pbuf.at[c, 2, low], relay.at[c, 1], r_ss.at[c, 1], r_rs.at[c, 1], left),
-            send(pbuf.at[c, 3, low], ring.at[c, 0, low], r_ss.at[c, 2], r_rs.at[c, 2], right),
-            send(pbuf.at[c, 1, high], ring.at[c, 1, high], r_ss.at[c, 3], r_rs.at[c, 3], left),
+            hop(pbuf, (c, 2), relay, (c, 0), high, r_ss, r_rs, 0, right),
+            hop(pbuf, (c, 2), relay, (c, 0), low, r_ss, r_rs, 1, left),
+            hop(pbuf, (c, 3), ring, (c, 0), low, r_ss, r_rs, 2, right),
+            hop(pbuf, (c, 1), ring, (c, 1), high, r_ss, r_rs, 3, left),
         ]
 
     def stage_join(c):
+        at_lanes = here(c)
         sums[c][0].wait_recv()
-        pbuf[c, 3, :HALF] = (
-            pbuf[c, 3, :HALF].astype(F32) + relay[c, 0].astype(F32)
+        pbuf[c, 3, :HALF, at_lanes] = (
+            pbuf[c, 3, :HALF, at_lanes].astype(F32) + relay[c, 0, :HALF, at_lanes].astype(F32)
         ).astype(BF)
-        one = send(pbuf.at[c, 3, high], ring.at[c, 0, high], r_ss.at[c, 4], r_rs.at[c, 4], right)
+        one = hop(pbuf, (c, 3), ring, (c, 0), high, r_ss, r_rs, 4, right)
         sums[c][1].wait_recv()
-        pbuf[c, 1, HALF:] = (
-            pbuf[c, 1, HALF:].astype(F32) + relay[c, 1].astype(F32)
+        pbuf[c, 1, HALF:, at_lanes] = (
+            pbuf[c, 1, HALF:, at_lanes].astype(F32) + relay[c, 0, HALF:, at_lanes].astype(F32)
         ).astype(BF)
-        two = send(pbuf.at[c, 1, low], ring.at[c, 1, low], r_ss.at[c, 5], r_rs.at[c, 5], left)
+        two = hop(pbuf, (c, 1), ring, (c, 1), low, r_ss, r_rs, 5, left)
         joined[c] = (one, two)
 
     def stage_sum(c):
         for copy in sums[c][2:] + list(joined[c]):
             copy.wait_recv()
-        ebuf[c] = (
-            pbuf[c, 0].astype(F32) + ring[c, 0].astype(F32) + ring[c, 1].astype(F32)
+        ebuf[c, :, here(c)] = (
+            pbuf[c, 0, :, here(c)].astype(F32)
+            + ring[c, 0, :, here(c)].astype(F32)
+            + ring[c, 1, :, here(c)].astype(F32)
         ).astype(BF)
         back_x[c] = over_x(
-            lambda c, s: ebuf.at[c, s], lambda c, s: xback.at[c, s], c, bl_sem, bx_ss, bx_rs
+            lambda c, s: ebuf.at[c, s, across_lanes(c)],
+            lambda c, s: xback.at[c, s, across_lanes(c)],
+            c,
+            bl_sem,
+            bx_ss,
+            bx_rs,
         )
 
     def stage_back(c):
         arrived(back_x[c])
-        zsend[c] = mm(order_back, xback[c]).astype(BF)
+        zsend[c, :, here(c)] = mm(order_back, xback[c, :, here(c)]).astype(BF)
         back_z[c] = over_z(zsend, zback, c, cl_sem, bz_ss, bz_rs)
 
     def stage_pick(c):
         arrived(back_z[c])
-        s = c // PARTS
-        part = share[0] * mm(picking(0, s), zback[c]) + share[1] * mm(picking(1, s), zback[c])
-        if s == 0:
-            branch_ref[:, lanes(c)] = part
-        else:
-            branch_ref[:, lanes(c)] += part
+        s = PIECES[c][0]
+        back = zback[c, :, here(c)]
+        branch_ref[:, lanes(c)] += share[0] * mm(picking(0, s), back) + share[1] * mm(
+            picking(1, s), back
+        )
 
     stages = {
         "z": stage_z,
@@ -694,14 +761,16 @@
     dma = pltpu.SemaphoreType.DMA
     vmem = pl.BlockSpec(memory_space=pltpu.VMEM)
     hbm = pl.BlockSpec(memory_space=pl.ANY)
-    buf = pltpu.VMEM((CHUNKS, ROWS, LANES), BF)
+    buf = pltpu.VMEM((CHUNKS, ROWS, WIDE), BF)
     return pl.pallas_call(
         layer_kernel,
         out_shape=jax.ShapeDtypeStruct((SUB, D), BF),
-        in_specs=[vmem] * 17 + [hbm] * 5,
+        in_specs=[vmem] * 7 + [hbm] * 5 + [vmem] * 5 + [hbm] * 5,
         out_specs=vmem,
         scratch_shapes=[
             pltpu.VMEM((SUB, D), F32),
+            pltpu.VMEM((2, 256, 128), BF),
+            pltpu.VMEM((SUB, D), BF),
             pltpu.VMEM((NX, TOK, 384), BF),
             pltpu.VMEM((NZ, NC, TOK + ROPE, 256), BF),
             pltpu.VMEM((256, 512), BF),
@@ -722,25 +791,25 @@
             buf,
             buf,
             buf,
-            pltpu.VMEM((CHUNKS, NT, ROWS, LANES), BF),
+            pltpu.VMEM((CHUNKS, NT, ROWS, WIDE), BF),
             pltpu.VMEM((D, 2 * HID), BF),
             pltpu.VMEM((HID, D), BF),
             pltpu.VMEM((NT * ROWS, 2 * HID), F32),
             pltpu.VMEM((NT * ROWS, HID), BF),
-            pltpu.VMEM((CHUNKS, NT, ROWS, LANES), BF),
-            pltpu.VMEM((CHUNKS, 2, HALF, LANES), BF),
-            pltpu.VMEM((CHUNKS, 2, ROWS, LANES), BF),
+            pltpu.VMEM((CHUNKS, NT, ROWS, WIDE), BF),
+            pltpu.VMEM((CHUNKS, 1, ROWS, WIDE), BF),
+            pltpu.VMEM((CHUNKS, 2, ROWS, WIDE), BF),
             buf,
             buf,
             buf,
             buf,
-            dma((5,)),
+            dma((10,)),
             dma((NX,)),
             dma((NX,)),
-            dma((5,)),
-            dma((5,)),
-            dma((5,)),
-            dma((5,)),
+            dma((5, 2)),
+            dma((5, 2)),
+            dma((5, 2)),
+            dma((5, 2)),
             dma((9,)),
             dma((9,)),
             dma((NX,)),

time: 136 us -> 135 us (level)
  no operation moved by 1% of the time
where the time goes in v4:
time: 135 us
  Pallas kernels  132 us (98%)
  local copies, waits for them, and re-layouts  1.67 us (1%)
    pallas_call x1, Pallas kernels, layer(): pl.pallas_call(layer_kernel, out_shape=jax.ShapeDtypeStruct((SUB, D), BF)...  132 us

profile of v4, /device:TPU:1, one launch (start us, length us, event | category | flops | bytes accessed | tf_op | source)
XLA Modules:
  0.0 135.0 jit_solution(5613310782040560799)
XLA Ops:
  0.0 0.8 multiply_sine_fusion
  0.8 132.5 %layer.1 = bf16[64,2048]{1,0:T(8,128)(2,1)} custom-call(bf16[256,256]{1,0:T(8,128)(2,1)} %latent.1, f32[1,256]{1,0:T(1,128)} %bitcast.13, bf16[64,256]{1,0:T(8,128)(2,1)} %bitcast.9, bf16[192,256]{1,0:T(8,128)(2,1)} %bitcast.8, bf16[256,128]{1,0:T(8,128)(2,1)} %narrow_q.1, f32[32,256]{1,0:T(8,128)} %get-tuple-element.6.cosine, ...), custom_call_target="tpu_custom_call" | custom-call | tf_op jit(solution)/shard_map/layer/pallas_call | solution.py:765
  133.3 1.7 %copy.22 = bf16[64,2048]{1,0:T(8,128)(2,1)} copy(bf16[64,2048]{1,0:T(8,128)(2,1)} %layer.1) | data formatting | bytes 524288
  (2 shorter events, 0.0 us)

commit v5 on v4

--- a/solution.py
+++ b/solution.py
@@ -439,13 +439,6 @@
         def _():
             forward(3)
 
-        @pl.when(j == 1)
-        def _():
-            wcopies[0].wait_recv()
-            wcopies[2].start()
-            wcopies[1].wait_recv()
-            wcopies[3].start()
-
         return carry
 
     lax.fori_loop(0, NX, second_body, 0)
@@ -485,6 +478,13 @@
 
     def last_body(i, carry):
         j = 2 + i - i // 2 * (2 * i - 1)
+        @pl.when(i == 1)
+        def _():
+            wcopies[0].wait_recv()
+            wcopies[2].start()
+            wcopies[1].wait_recv()
+            wcopies[3].start()
+
         attend(j, 3, False)
         finish(j)
         for other in range(1, NX):

time: 135 us -> 134 us (level)
  no operation moved by 1% of the time
where the time goes in v5:
time: 134 us
  Pallas kernels  132 us (99%)
  local copies, waits for them, and re-layouts  1.67 us (1%)
    pallas_call x1, Pallas kernels, layer(): pl.pallas_call(layer_kernel, out_shape=jax.ShapeDtypeStruct((SUB, D), BF)...  132 us

profile of v5, /device:TPU:1, one launch (start us, length us, event | category | flops | bytes accessed | tf_op | source)
XLA Modules:
  0.0 134.3 jit_solution(5328035640234358010)
XLA Ops:
  0.0 0.8 multiply_sine_fusion
  0.8 131.8 %layer.1 = bf16[64,2048]{1,0:T(8,128)(2,1)} custom-call(bf16[256,256]{1,0:T(8,128)(2,1)} %latent.1, f32[1,256]{1,0:T(1,128)} %bitcast.13, bf16[64,256]{1,0:T(8,128)(2,1)} %bitcast.9, bf16[192,256]{1,0:T(8,128)(2,1)} %bitcast.8, bf16[256,128]{1,0:T(8,128)(2,1)} %narrow_q.1, f32[32,256]{1,0:T(8,128)} %get-tuple-element.6.cosine, ...), custom_call_target="tpu_custom_call" | custom-call | tf_op jit(solution)/shard_map/layer/pallas_call | solution.py:765
  132.7 1.7 %copy.22 = bf16[64,2048]{1,0:T(8,128)(2,1)} copy(bf16[64,2048]{1,0:T(8,128)(2,1)} %layer.1) | data formatting | bytes 524288
  (2 shorter events, 0.0 us)
